TPU v7x, 512 devices: a whole 4x4x16 slice. The times are simulated.
512 devices in a mesh: sp: 16 (over z), dp: 32 (over y, x, core).
Axes of the slice: x: 4, y: 4, z: 16, core: 2. Of those that a mesh axis runs over, the one named last changes fastest.
Arguments:
- up_pre: bfloat16 [32, 6144, 2048], P('dp', 'sp'), may hold values from -6 to 6
- mix_pre: bfloat16 [32, 6144, 2048], P('dp', 'sp'), may hold values from -6 to 6
- ln_gain: float32 [2048], replicated, may hold values from 0.1 to 1.9
- mix_weight: bfloat16 [16, 128, 128], replicated, may hold values from -0.5 to 0.5
- mix_bias: float32 [16, 128], replicated, may hold values from 0.1 to 1.9
- out_weight: bfloat16 [2048, 2048], P('sp', 'dp'), may hold values from -0.125 to 0.125
Outputs:
- mixed_out: bfloat16 [32, 6144, 2048], P('dp', 'sp')
All inputs are finite; a program needn't handle non-finite values.
Results may differ from a plain program's by a relative error of at most 0.012.
Values may be sent and summed in bfloat16 or wider, within the bound.
No kernel may reach another device: no remote copies, remote signals or barrier semaphores. Data moves between devices by JAX's collectives and lax.ppermute only.
A program may use at most 64 MiB of HBM per device.

v0:
```python
import jax
import jax.numpy as jnp
from jax import lax
from jax.sharding import PartitionSpec as P

BLOCK = 128


norm_epsilon = 1e-05


def sent_to_all(value, axis):
    length = lax.axis_size(axis)
    return lax.all_to_all(
        jnp.broadcast_to(value[None], (length, *value.shape)), axis, 0, 0, tiled=True
    )


def joined_along(tiles, dim):
    lengths = list(tiles.shape[1:])
    lengths[dim] *= tiles.shape[0]
    return jnp.moveaxis(tiles, 0, dim).reshape(lengths)


def gather_directly(value, axis, dim):
    tiles = sent_to_all(value, axis)
    return joined_along(tiles, dim)


def normalize(up_rows, mix_rows, ln_gain):
    up_act = jax.nn.gelu(up_rows.astype(jnp.float32), approximate=False).astype(jnp.bfloat16)
    activated = jax.nn.gelu(mix_rows.astype(jnp.float32), approximate=False)
    center = jnp.mean(activated, axis=-1, keepdims=True)
    spread = jnp.mean(jnp.square(activated - center), axis=-1, keepdims=True)
    normed = ((activated - center) * lax.rsqrt(spread + norm_epsilon) * ln_gain).astype(
        jnp.bfloat16
    )
    return (up_act, normed)


def mix_blocks(up_act, normed, local_weight, local_bias):
    row_count, channels = normed.shape
    local_groups = local_weight.shape[0]
    blocks = normed.reshape(row_count // BLOCK, BLOCK, local_groups, channels // local_groups)
    mixed_sum = jnp.einsum(
        "gts,nsgc->ntgc", local_weight, blocks, preferred_element_type=jnp.float32
    )
    mixed_sum = mixed_sum + jnp.transpose(local_bias)[None, :, :, None]
    return (up_act.astype(jnp.float32) * mixed_sum.reshape(row_count, channels)).astype(
        jnp.bfloat16
    )


def per_device(up_pre, mix_pre, ln_gain, mix_weight, mix_bias, out_weight):
    up_act, normed = normalize(up_pre[0], mix_pre[0], ln_gain)
    positions = lax.broadcasted_iota(jnp.int32, (BLOCK, BLOCK), 0)
    sources = lax.broadcasted_iota(jnp.int32, (BLOCK, BLOCK), 1)
    causal = positions >= sources
    masked = jnp.where(causal[None], mix_weight, jnp.zeros_like(mix_weight))
    gated = mix_blocks(up_act, normed, masked, mix_bias)
    rows_whole = gather_directly(out_weight, "sp", 0)
    result = jnp.dot(
        gated,
        lax.all_gather(rows_whole, "dp", axis=1, tiled=True),
        preferred_element_type=jnp.float32,
    )
    return result.astype(jnp.bfloat16)[None]


def solution(mesh):
    return jax.shard_map(
        per_device,
        mesh=mesh,
        in_specs=(P("dp", "sp", None), P("dp", "sp", None), P(), P(), P(), P("sp", "dp")),
        out_specs=P("dp", "sp", None),
        check_vma=False,
    )
```

profile of v0, /device:TPU:1, one launch (start us, length us, event | category | flops | bytes accessed | tf_op | source)
XLA Modules:
  0.0 127.7 jit_solution(11974662628502743535)
XLA Ops:
  6.5 0.0 all-gather.2.cloned.1.call-start
  6.5 0.8 broadcast_in_dim.16
  7.3 29.3 %all_to_all.5 = bf16[16,128,64]{1,2,0:T(8,128)(2,1)S(1)} all-to-all(bf16[16,128,64]{1,2,0:T(8,128)(2,1)S(1)} %broadcast_in_dim.16), channel_id=1, replica_groups=mesh['sp'=16,'dp'=32] {'sp'}, dimensions={0} | all-to-all | bytes 524288 | tf_op jit(solution)/shard_map/all_to_all | solution.py:14
  36.6 0.7 copy_bitcast_fusion
  37.3 0.0 all-gather.2.cloned.1.call-update
  37.4 3.6 %fusion.38 = (f32[48,8,16,128]{3,1,2,0:T(8,128)S(1)}, f32[48,8,16,128]{3,1,2,0:T(8,128)}) fusion(bf16[1,384,2048]{2,1,0:T(8,128)(2,1)} %param.7), kind=kLoop, calls=%fused_computation.45 | loop fusion | flops 3145728 | bytes 7864320
  41.0 0.7 copy.40
  41.6 2.4 %copy.29 = f32[3,128,16,128]{1,3,0,2:T(8,128)} copy(f32[3,128,16,128]{3,2,1,0:T(8,128)S(1)} %bitcast.232) | data formatting | bytes 6291456 | tf_op jit(solution)/shard_map/mul | solution.py:32
  44.1 2.5 %copy.39 = f32[48,8,16,128]{3,2,1,0:T(8,128)S(1)} copy(f32[48,8,16,128]{3,1,2,0:T(8,128)} %get-tuple-element.8) | data formatting | bytes 6291456
  46.6 2.4 %copy.34 = f32[3,128,16,128]{1,3,0,2:T(8,128)} copy(f32[3,128,16,128]{3,2,1,0:T(8,128)S(1)} %bitcast.233) | data formatting | bytes 6291456 | tf_op jit(solution)/shard_map/mul | solution.py:32
  49.1 0.0 copy-start
  49.1 0.0 copy-start.1
  49.1 0.0 copy-start.2
  49.1 0.0 copy-start.3
  49.1 0.0 copy-start.4
  49.1 8.6 %fusion.177 = (f32[384]{0:T(512)S(1)}, f32[384,2048]{1,0:T(8,128)S(1)}) fusion(bf16[1,384,2048]{2,1,0:T(8,128)(2,1)} %param.7), kind=kLoop, calls=%fused_computation.197 | loop fusion | flops 51904128 | bytes 4720128 | tf_op jit(solution)/shard_map/reduce_sum | solution.py:33
  57.8 0.5 multiply_reduce_fusion
  58.2 0.0 copy-done
  58.2 0.0 copy-done.1
  58.3 0.0 copy-done.2
  58.3 8.6 %bitcast_add_fusion = f32[3,128,16,128]{1,3,0,2:T(8,128)} fusion(f32[128,16]{0,1:T(8,128)S(1)} %bitcast.235, f32[3,128,16,128]{1,3,0,2:T(8,128)S(1)} %copy-done.1, f32[3,128,16,128]{1,3,0,2:T(8,128)S(1)} %copy-done, f32[16,128]{1,0:T(8,128)S(1)} %bitcast.236, f32[3,128]{1,0:T(4,128)S(1)} %rsqrt_bitcast_fusion, f32[3,128]{1,0:T(4,128)S(1)} %get-tuple-element.9, ...), kind=kOutput, calls=%fused_computation.82 | convolution fusion | flops 253493248 | bytes 9997312 | tf_op jit(solution)/shard_map/gts,nsgc->ntgc/dot_general | solution.py:45
  66.9 2.8 %copy.35 = f32[3,128,16,128]{3,2,1,0:T(8,128)S(1)} copy(f32[3,128,16,128]{1,3,0,2:T(8,128)} %bitcast_add_fusion) | data formatting | bytes 6291456 | tf_op jit(solution)/shard_map/add | solution.py:48
  69.6 36.3 %all-gather.2.cloned.1.call-done = bf16[2048,2048]{0,1:T(8,128)(2,1)} async-done(((bf16[2048,64]{0,1:T(8,128)(2,1)}), bf16[2048,2048]{0,1:T(8,128)(2,1)}) %all-gather.2.cloned.1.call-update) | async-done | bytes 8388624 | tf_op jit(solution)/shard_map/all_gather | solution.py:64
  106.0 14.9 %fusion.80 = bf16[1,384,2048]{2,1,0:T(8,128)(2,1)} fusion(bf16[2048,2048]{0,1:T(8,128)(2,1)} %all-gather.2.cloned.1.call-done, f32[48,8,16,128]{3,2,1,0:T(8,128)S(1)} %bitcast.234, bf16[1,384,2048]{2,1,0:T(8,128)(2,1)} %param.6), kind=kOutput, calls=%fused_computation.98 | convolution fusion | flops 3276275712 | bytes 14680064 | tf_op jit(solution)/shard_map/dot_general | solution.py:62
  (5 shorter events, 0.0 us)
Async XLA Ops:
  6.5 99.4 %all-gather.2.cloned.1.call-start = ((), (), s32[]{:S(2)}) async-start(), calls=%async_computation.1 | async-start | bytes 8650752 | tf_op jit(solution)/shard_map/all_gather | solution.py:64
  49.1 9.2 %copy-start = (f32[3,128,16,128]{1,3,0,2:T(8,128)S(1)}, f32[3,128,16,128]{1,3,0,2:T(8,128)}, u32[]{:S(2)}) copy-start(f32[3,128,16,128]{1,3,0,2:T(8,128)} %copy.29) | copy-start | bytes 9437188
  49.1 9.2 %copy-start.1 = (f32[3,128,16,128]{1,3,0,2:T(8,128)S(1)}, f32[3,128,16,128]{1,3,0,2:T(8,128)}, u32[]{:S(2)}) copy-start(f32[3,128,16,128]{1,3,0,2:T(8,128)} %copy.34) | copy-start | bytes 9437188
  49.1 9.2 %copy-start.2 = (bf16[16,128,128]{2,1,0:T(8,128)(2,1)S(1)}, bf16[16,128,128]{2,1,0:T(8,128)(2,1)}, u32[]{:S(2)}) copy-start(bf16[16,128,128]{2,1,0:T(8,128)(2,1)} %param.9) | copy-start | bytes 1572868
  49.1 9.2 %copy-start.3 = (f32[16,128]{1,0:T(8,128)S(1)}, f32[16,128]{1,0:T(8,128)}, u32[]{:S(2)}) copy-start(f32[16,128]{1,0:T(8,128)} %param.10) | copy-start | bytes 24580
  49.1 9.2 %copy-start.4 = (f32[2048]{0:T(1024)S(1)}, f32[2048]{0:T(1024)}, u32[]{:S(2)}) copy-start(f32[2048]{0:T(1024)} %param.8) | copy-start | bytes 24580
Sparse Core Ops, SparseCore 0:
  37.5 68.4 all-gather.1
where the time goes:
time: 128 us
  waiting for transfers between devices  36.3 us (28%)
  blocking collectives  29.3 us (23%)
  matrix products  23.5 us (18%)
  between operations  13.5 us (11%)
  other arithmetic  12.7 us (10%)
  local copies, waits for them, and re-layouts  12.4 us (10%)
    all_gather x1, waiting for transfers between devices, per_device(): lax.all_gather(rows_whole, 'dp', axis=1, tiled=True)  36.3 us
    all_to_all x1, blocking collectives, sent_to_all(): lax.all_to_all(jnp.broadcast_to(value[None], (length, *value.shape)), axi...  29.3 us
    dot_general x1, matrix products, per_device(): jnp.dot(gated, lax.all_gather(rows_whole, 'dp', axis=1, tiled=True), pref...  14.9 us
    reduce_sum x1, other arithmetic, normalize(): center = jnp.mean(activated, axis=-1, keepdims=True)  8.64 us
    dot_general x1, matrix products, mix_blocks(): jnp.einsum('gts,nsgc->ntgc', local_weight, blocks, preferred_element_type...  8.58 us
    mul x2, local copies, waits for them, and re-layouts, normalize(): activated = jax.nn.gelu(mix_rows.astype(jnp.float32), approximate=False)  4.87 us
    unnamed x1, other arithmetic  3.59 us
    unnamed x12, local copies, waits for them, and re-layouts  3.22 us
  transfers between devices with their start and end apart: 1, of which 1 were waited for; matrix products, arithmetic and copies ran while one was open for 25% of the time, Pallas kernels for 0%

commit v1 on v0

v1 whole, which is shorter than its diff:
```python
import functools

import jax
import jax.numpy as jnp
from jax import lax
from jax.experimental import pallas as pl
from jax.experimental.pallas import tpu as pltpu
from jax.sharding import PartitionSpec as P

BLOCK = 128
norm_epsilon = 1e-05
HALF_ROOT = 0.7071067811865476
BF = jnp.bfloat16
F32 = jnp.float32


def gelu(x):
    return (0.5 * x) * (1.0 + lax.erf(x * HALF_ROOT))


def norm_kernel(mix_ref, gain_ref, out_ref, act_ref):
    rows, width = mix_ref.shape
    step = 16

    def body(i, _):
        at = pl.ds(pl.multiple_of(i * step, step), step)
        act = gelu(mix_ref[at, :].astype(F32))
        act_ref[at, :] = act
        center = jnp.sum(act, axis=-1, keepdims=True) * (1.0 / width)
        off = act - center
        spread = jnp.sum(off * off, axis=-1, keepdims=True) * (1.0 / width)
        scale = lax.rsqrt(spread + norm_epsilon)
        out_ref[at, :] = ((act_ref[at, :] - center) * scale * gain_ref[...]).astype(BF)
        return 0

    lax.fori_loop(0, rows // step, body, 0, unroll=2)


def norm(mix, gain):
    rows, width = mix.shape
    return pl.pallas_call(
        norm_kernel,
        grid=(rows // BLOCK,),
        in_specs=[
            pl.BlockSpec((BLOCK, width), lambda i: (i, 0)),
            pl.BlockSpec((1, width), lambda i: (0, 0)),
        ],
        out_specs=pl.BlockSpec((BLOCK, width), lambda i: (i, 0)),
        out_shape=jax.ShapeDtypeStruct((rows, width), BF),
        scratch_shapes=[pltpu.VMEM((BLOCK, width), F32)],
        compiler_params=pltpu.CompilerParams(vmem_limit_bytes=8 << 20),
        cost_estimate=pl.CostEstimate(
            flops=4_000_000_000, bytes_accessed=rows * width * 4, transcendentals=rows * width
        ),
        name="norm",
    )(mix, gain)


def gate_kernel(normed_ref, up_ref, weight_ref, bias_ref, out_ref):
    groups, block, _ = weight_ref.shape
    width = up_ref.shape[1] // groups
    keep = lax.broadcasted_iota(jnp.int32, (block, block), 0) >= lax.broadcasted_iota(
        jnp.int32, (block, block), 1
    )
    for g in range(groups):
        cols = slice(g * width, (g + 1) * width)
        masked = jnp.where(keep, weight_ref[g].astype(F32), 0.0).astype(BF)
        mixed = jnp.dot(masked, normed_ref[:, cols], preferred_element_type=F32)
        mixed = mixed + bias_ref[:, g : g + 1]
        up = gelu(up_ref[:, cols].astype(F32)).astype(BF).astype(F32)
        out_ref[:, cols] = (up * mixed).astype(BF)


def gate(normed, up, weight, bias_t):
    rows, width = up.shape
    groups = weight.shape[0]
    return pl.pallas_call(
        gate_kernel,
        grid=(rows // BLOCK,),
        in_specs=[
            pl.BlockSpec((BLOCK, width), lambda i: (i, 0)),
            pl.BlockSpec((BLOCK, width), lambda i: (i, 0)),
            pl.BlockSpec((groups, BLOCK, BLOCK), lambda i: (0, 0, 0)),
            pl.BlockSpec((BLOCK, groups), lambda i: (0, 0)),
        ],
        out_specs=pl.BlockSpec((BLOCK, width), lambda i: (i, 0)),
        out_shape=jax.ShapeDtypeStruct((rows, width), BF),
        compiler_params=pltpu.CompilerParams(vmem_limit_bytes=8 << 20),
        cost_estimate=pl.CostEstimate(
            flops=4_000_000_000, bytes_accessed=rows * width * 6, transcendentals=rows * width
        ),
        name="gate",
    )(normed, up, weight, bias_t)


def project_kernel(gated_ref, *refs):
    own, other, out_ref = refs[:5], refs[5:10], refs[10]
    index = lax.axis_index("dp")
    core, x, y = index & 1, (index >> 1) & 3, index >> 3
    first, second = lax.select(core == 0, x, y), lax.select(core == 0, y, x)
    blocks = own[0].shape[1]
    half = blocks // 2
    pair = 2 * own[0].shape[2]

    def tile(refs, r, j, k):
        if r == 2:
            return refs[3][j, k] if k < half else refs[4][j, k - half]
        return refs[(0, 1, None, 2)[r]][j, k]

    for r in range(4):
        a = lax.rem(first + r, 4)
        for s in range(0, 4, 2):
            rhs = []
            at = []
            for t in (s, s + 1):
                b = lax.rem(second + t, 4)
                at.append(lax.select(core == 0, b * 4 + a, a * 4 + b))
                rhs.append([tile(own, r, b, k) for k in range(blocks)])
                rhs.append([tile(other, t, a, k) for k in range(blocks)])
            whole = jnp.concatenate([jnp.concatenate(x, axis=1) for x in rhs], axis=0)
            result = lax.dot_general(
                gated_ref[...], whole, (((1,), (1,)), ((), ())), preferred_element_type=F32
            )
            for n in range(2):
                part = pltpu.roll(result[:, n * pair : (n + 1) * pair], core * (pair // 2), 1)
                where = pl.ds(pl.multiple_of(at[n] * pair, pair), pair)
                out_ref[:, where] = part.astype(BF)


def project(gated, own, other):
    rows = gated.shape[0]
    width = 16 * 2 * own[0].shape[2]
    vmem = pl.BlockSpec(memory_space=pltpu.VMEM)
    return pl.pallas_call(
        project_kernel,
        in_specs=[vmem] * 11,
        out_specs=vmem,
        out_shape=jax.ShapeDtypeStruct((rows, width), BF),
        compiler_params=pltpu.CompilerParams(vmem_limit_bytes=6 << 20),
        cost_estimate=pl.CostEstimate(
            flops=2 * rows * width * gated.shape[1], bytes_accessed=12 << 20, transcendentals=0
        ),
        name="project",
    )(gated, *own, *other)


def at(y, x, core):
    return (y % 4 * 4 + x % 4) * 2 + core


GROUPS = [[at(y, x, 0) for y in range(4)] for x in range(4)] + [
    [at(y, x, 1) for x in range(4)] for y in range(4)
]


def ring(shift):
    pairs = []
    for y in range(4):
        for x in range(4):
            pairs.append((at(y, x, 0), at(y, x + shift, 0)))
            pairs.append((at(y, x, 1), at(y + shift, x, 1)))
    return pairs


SWAP = [(d, d ^ 1) for d in range(32)]


def sent_to_all(value, axis, length, groups=None):
    return lax.all_to_all(
        jnp.broadcast_to(value[None], (length, *value.shape)),
        axis,
        0,
        0,
        tiled=True,
        axis_index_groups=groups,
    )


def per_device(up_pre, mix_pre, ln_gain, mix_weight, mix_bias, out_weight):
    slab = sent_to_all(out_weight.T, "sp", 16)
    normed = norm(mix_pre[0], ln_gain[None])
    slab, normed = lax.optimization_barrier((slab, normed))
    own = sent_to_all(slab, "dp", 4, GROUPS)
    gated = gate(normed, up_pre[0], mix_weight, mix_bias.T)
    own, gated = lax.optimization_barrier((own, gated))
    before = lax.ppermute(own, "dp", ring(1))
    after = lax.ppermute(own, "dp", ring(-1))
    other = lax.ppermute(own, "dp", SWAP)
    before, after, other = lax.optimization_barrier((before, after, other))
    far_low = lax.ppermute(before[:, :8], "dp", ring(1))
    far_high = lax.ppermute(after[:, 8:], "dp", ring(-1))
    mine = [own, after, before, far_low, far_high]
    theirs = [other] + [lax.ppermute(v, "dp", SWAP) for v in mine[1:]]
    return project(gated, mine, theirs)[None]


def solution(mesh):
    return jax.shard_map(
        per_device,
        mesh=mesh,
        in_specs=(P("dp", "sp", None), P("dp", "sp", None), P(), P(), P(), P("sp", "dp")),
        out_specs=P("dp", "sp", None),
        check_vma=False,
    )
```

time: 128 us -> 101 us (0.79)
  starting transfers between devices: 0.01 us -> 53 us
  blocking collectives: 29.3 us -> 0 us
  matrix products: 23.5 us -> 0 us
  between operations: 13.5 us -> 0.2 us
  other arithmetic: 12.7 us -> 0 us
  Pallas kernels: 0 us -> 9.54 us
  waiting for transfers between devices: 36.3 us -> 29.4 us
  local copies, waits for them, and re-layouts: 12.4 us -> 8.67 us
    all_gather x1 -> x0, waiting for transfers between devices: 36.3 us -> none  [per_device(): lax.all_gather(rows_whole, 'dp', axis=1, tiled=True)]
    ppermute x0 -> x9, starting transfers between devices: none -> 33.2 us  [the longest x4 12.3 us: per_device(): theirs = [other] + [lax.ppermute(v, 'dp', SWAP) for v in mine[1:]]]
    all_to_all x1 -> x0, blocking collectives: 29.3 us -> none  [sent_to_all(): lax.all_to_all(jnp.broadcast_to(value[None], (length, *value.shape)), axi...]
    dot_general x2 -> x0, matrix products: 23.5 us -> none  [the longest x1 14.9 us: per_device(): jnp.dot(gated, lax.all_gather(rows_whole, 'dp', axis=1, tiled=True), pref...]
    all_to_all x0 -> x2, starting transfers between devices: none -> 19.7 us  [sent_to_all(): lax.all_to_all(jnp.broadcast_to(value[None], (length, *value.shape)), axi...]
    ppermute x0 -> x9, waiting for transfers between devices: none -> 16.4 us  [the longest x1 10.5 us: per_device(): after = lax.ppermute(own, 'dp', ring(-1))]
    all_to_all x0 -> x2, waiting for transfers between devices: none -> 13 us  [sent_to_all(): lax.all_to_all(jnp.broadcast_to(value[None], (length, *value.shape)), axi...]
    pallas_call x0 -> x3, Pallas kernels: none -> 9.54 us  [the longest x1 4.99 us: project(): pl.pallas_call(project_kernel, in_specs=[vmem] * 11, out_specs=vmem, out_...]
  transfers between devices with their start and end apart: 1 -> 11, of which waited for: 1 -> 5; matrix products, arithmetic and copies ran while one was open for 25% -> 0% of each run, Pallas kernels for 0% -> 5%
where the time goes in v1:
time: 101 us
  starting transfers between devices  53 us (52%)
  waiting for transfers between devices  29.4 us (29%)
  Pallas kernels  9.54 us (9%)
  local copies, waits for them, and re-layouts  8.67 us (9%)
    all_to_all x2, starting transfers between devices, sent_to_all(): lax.all_to_all(jnp.broadcast_to(value[None], (length, *value.shape)), axi...  19.7 us
    all_to_all x2, waiting for transfers between devices, sent_to_all(): lax.all_to_all(jnp.broadcast_to(value[None], (length, *value.shape)), axi...  13 us
    ppermute x4, starting transfers between devices, per_device(): theirs = [other] + [lax.ppermute(v, 'dp', SWAP) for v in mine[1:]]  12.3 us
    ppermute x1, waiting for transfers between devices, per_device(): after = lax.ppermute(own, 'dp', ring(-1))  10.5 us
    ppermute x1, starting transfers between devices, per_device(): other = lax.ppermute(own, 'dp', SWAP)  9.19 us
    unnamed x19, local copies, waits for them, and re-layouts  5.89 us
    pallas_call x1, Pallas kernels, project(): pl.pallas_call(project_kernel, in_specs=[vmem] * 11, out_specs=vmem, out_...  4.99 us
    ppermute x1, starting transfers between devices, per_device(): far_high = lax.ppermute(after[:, 8:], 'dp', ring(-1))  4.57 us
  transfers between devices with their start and end apart: 11, of which 5 were waited for; matrix products, arithmetic and copies ran while one was open for 0% of the time, Pallas kernels for 5%

profile of v1, /device:TPU:1, one launch (start us, length us, event | category | flops | bytes accessed | tf_op | source)
XLA Modules:
  0.0 100.8 jit_solution(12130808031389565165)
XLA Ops:
  0.0 1.5 %broadcast_in_dim.8 = bf16[16,64,128]{2,1,0:T(8,128)(2,1)} broadcast(bf16[64,128]{1,0:T(8,128)(2,1)} %bitcast.10), dimensions={1,2} | broadcast | bytes 278528 | tf_op jit(solution)/shard_map/broadcast_in_dim | solution.py:170
  1.5 15.7 %all-to-all-start = ((bf16[16,64,128]{2,1,0:T(8,128)(2,1)}), bf16[16,64,128]{2,1,0:T(8,128)(2,1)S(1)}, u32[]{:S(2)}, u32[]{:S(2)}) async-start(bf16[16,64,128]{2,1,0:T(8,128)(2,1)} %broadcast_in_dim.8), calls=%async_computation | async-start | bytes 524288 | tf_op jit(solution)/shard_map/all_to_all | solution.py:169
  17.2 1.4 %copy-done = bf16[1,384,2048]{2,1,0:T(8,128)(2,1)S(1)} copy-done((bf16[1,384,2048]{2,1,0:T(8,128)(2,1)S(1)}, bf16[1,384,2048]{2,1,0:T(8,128)(2,1)}, u32[]{:S(2)}) %copy-start) | copy-done | bytes 1572888
  19.3 3.1 %norm.1.normed_ref = bf16[384,2048]{1,0:T(8,128)(2,1)S(1)} custom-call(bf16[384,2048]{1,0:T(8,128)(2,1)S(1)} %bitcast.7, f32[1,2048]{1,0:T(1,128)S(1)} %bitcast.9), custom_call_target="tpu_custom_call" | custom-call | flops 4000000000 | bytes 3145728 | tf_op jit(solution)/shard_map/norm/pallas_call | solution.py:41
  22.4 1.1 %copy-done.6 = bf16[384,2048]{1,0:T(8,128)(2,1)} copy-done((bf16[384,2048]{1,0:T(8,128)(2,1)}, bf16[384,2048]{1,0:T(8,128)(2,1)S(1)}, u32[]{:S(2)}) %copy-start.6) | copy-done | bytes 1572888
  23.5 7.4 %all-to-all-done = bf16[16,64,128]{2,1,0:T(8,128)(2,1)S(1)} async-done(((bf16[16,64,128]{2,1,0:T(8,128)(2,1)}), bf16[16,64,128]{2,1,0:T(8,128)(2,1)S(1)}, u32[]{:S(2)}, u32[]{:S(2)}) %all-to-all-start) | async-done | bytes 262176 | tf_op jit(solution)/shard_map/all_to_all | solution.py:169
  31.0 1.2 %broadcast_in_dim.20 = bf16[4,16,64,128]{3,2,1,0:T(8,128)(2,1)} broadcast(bf16[16,64,128]{2,1,0:T(8,128)(2,1)S(1)} %all-to-all-done), dimensions={1,2,3} | broadcast | bytes 1310720 | tf_op jit(solution)/shard_map/broadcast_in_dim | solution.py:170
  32.2 4.0 %all-to-all-start.1 = ((bf16[4,16,64,128]{3,2,1,0:T(8,128)(2,1)}), bf16[4,16,64,128]{3,2,1,0:T(8,128)(2,1)S(1)}, u32[]{:S(2)}, u32[]{:S(2)}) async-start(bf16[4,16,64,128]{3,2,1,0:T(8,128)(2,1)} %broadcast_in_dim.20), calls=%async_computation.1 | async-start | bytes 2097152 | tf_op jit(solution)/shard_map/all_to_all | solution.py:169
  36.4 1.4 %copy-done.7 = bf16[384,2048]{1,0:T(8,128)(2,1)S(1)} copy-done((bf16[384,2048]{1,0:T(8,128)(2,1)S(1)}, bf16[384,2048]{1,0:T(8,128)(2,1)}, u32[]{:S(2)}) %copy-start.7) | copy-done | bytes 1572888
  37.8 1.5 %gate.1.gated_ref = bf16[384,2048]{1,0:T(8,128)(2,1)S(1)} custom-call(bf16[384,2048]{1,0:T(8,128)(2,1)S(1)} %copy-done.7, bf16[384,2048]{1,0:T(8,128)(2,1)S(1)} %bitcast.8, bf16[16,128,128]{2,1,0:T(8,128)(2,1)S(1)} %copy-done.2, f32[128,16]{1,0:T(8,128)S(1)} %bitcast.6), custom_call_target="tpu_custom_call" | custom-call | flops 4000000000 | bytes 4718592 | tf_op jit(solution)/shard_map/gate/pallas_call | solution.py:77
  40.4 5.6 %all-to-all-done.1.refs_0_ = bf16[4,16,64,128]{3,2,1,0:T(8,128)(2,1)S(1)} async-done(((bf16[4,16,64,128]{3,2,1,0:T(8,128)(2,1)}), bf16[4,16,64,128]{3,2,1,0:T(8,128)(2,1)S(1)}, u32[]{:S(2)}, u32[]{:S(2)}) %all-to-all-start.1) | async-done | bytes 1048608 | tf_op jit(solution)/shard_map/all_to_all | solution.py:169
  46.0 9.2 %collective-permute-start.2 = (bf16[4,16,64,128]{3,2,1,0:T(8,128)(2,1)S(1)}, bf16[4,16,64,128]{3,2,1,0:T(8,128)(2,1)S(1)}, u32[]{:S(2)}, u32[]{:S(2)}) collective-permute-start(bf16[4,16,64,128]{3,2,1,0:T(8,128)(2,1)S(1)} %all-to-all-done.1.refs_0_), channel_id=1, source_target_pairs={{0,1},{1,0},{2,3},{3,2},{4,5},{5,4},{6,7},{7,6},{8,9},{9,8},{10,11... | collective-permute-start | bytes 3145736 | tf_op jit(solution)/shard_map/ppermute | solution.py:188
  55.2 2.8 %collective-permute-start.1 = (bf16[4,16,64,128]{3,2,1,0:T(8,128)(2,1)S(1)}, bf16[4,16,64,128]{3,2,1,0:T(8,128)(2,1)S(1)}, u32[]{:S(2)}, u32[]{:S(2)}) collective-permute-start(bf16[4,16,64,128]{3,2,1,0:T(8,128)(2,1)S(1)} %all-to-all-done.1.refs_0_), channel_id=1, source_target_pairs={{0,6},{1,25},{2,0},{3,27},{4,2},{5,29},{6,4},{7,31},{8,14},{9,1},{... | collective-permute-start | bytes 3145736 | tf_op jit(solution)/shard_map/ppermute | solution.py:187
  58.0 2.5 %collective-permute-start = (bf16[4,16,64,128]{3,2,1,0:T(8,128)(2,1)S(1)}, bf16[4,16,64,128]{3,2,1,0:T(8,128)(2,1)S(1)}, u32[]{:S(2)}, u32[]{:S(2)}) collective-permute-start(bf16[4,16,64,128]{3,2,1,0:T(8,128)(2,1)S(1)} %all-to-all-done.1.refs_0_), channel_id=1, source_target_pairs={{0,2},{1,9},{2,4},{3,11},{4,6},{5,13},{6,0},{7,15},{8,10},{9,17},{... | collective-permute-start | bytes 3145736 | tf_op jit(solution)/shard_map/ppermute | solution.py:186
  60.5 10.5 %collective-permute-done.1.refs_1_ = bf16[4,16,64,128]{3,2,1,0:T(8,128)(2,1)S(1)} collective-permute-done((bf16[4,16,64,128]{3,2,1,0:T(8,128)(2,1)S(1)}, bf16[4,16,64,128]{3,2,1,0:T(8,128)(2,1)S(1)}, u32[]{:S(2)}, u32[]{:S(2)}) %collective-permute-start.1) | collective-permute-done | bytes 1048608 | tf_op jit(solution)/shard_map/ppermute | solution.py:187
  71.0 4.0 %collective-permute-done.refs_2_ = bf16[4,16,64,128]{3,2,1,0:T(8,128)(2,1)S(1)} collective-permute-done((bf16[4,16,64,128]{3,2,1,0:T(8,128)(2,1)S(1)}, bf16[4,16,64,128]{3,2,1,0:T(8,128)(2,1)S(1)}, u32[]{:S(2)}, u32[]{:S(2)}) %collective-permute-start) | collective-permute-done | bytes 1048608 | tf_op jit(solution)/shard_map/ppermute | solution.py:186
  75.1 1.9 %collective-permute-start.3 = (bf16[4,8,64,128]{3,2,1,0:T(8,128)(2,1)S(1)}, bf16[4,8,64,128]{3,2,1,0:T(8,128)(2,1)S(1)}, u32[]{:S(2)}, u32[]{:S(2)}) collective-permute-start(bf16[4,8,64,128]{3,2,1,0:T(8,128)(2,1)S(1)} %slice.6), channel_id=1, source_target_pairs={{0,2},{1,9},{2,4},{3,11},{4,6},{5,13},{6,0},{7,15},{8,10},{9,17},{... | collective-permute-start | bytes 1572872 | tf_op jit(solution)/shard_map/ppermute | solution.py:190
  77.0 4.6 %collective-permute-start.4 = (bf16[4,8,64,128]{3,2,1,0:T(8,128)(2,1)S(1)}, bf16[4,8,64,128]{3,2,1,0:T(8,128)(2,1)S(1)}, u32[]{:S(2)}, u32[]{:S(2)}) collective-permute-start(bf16[4,8,64,128]{3,2,1,0:T(8,128)(2,1)S(1)} %slice.7), channel_id=1, source_target_pairs={{0,6},{1,25},{2,0},{3,27},{4,2},{5,29},{6,4},{7,31},{8,14},{9,1},{... | collective-permute-start | bytes 1572872 | tf_op jit(solution)/shard_map/ppermute | solution.py:191
  81.6 5.2 %collective-permute-start.5 = (bf16[4,16,64,128]{3,2,1,0:T(8,128)(2,1)S(1)}, bf16[4,16,64,128]{3,2,1,0:T(8,128)(2,1)S(1)}, u32[]{:S(2)}, u32[]{:S(2)}) collective-permute-start(bf16[4,16,64,128]{3,2,1,0:T(8,128)(2,1)S(1)} %collective-permute-done.1.refs_1_), channel_id=1, source_target_pairs={{0,1},{1,0},{2,3},{3,2},{4,5},{5,4},{6,7},{7,6},{8,9},{9,8},{10,11... | collective-permute-start | bytes 3145736 | tf_op jit(solution)/shard_map/ppermute | solution.py:193
  86.8 1.9 %collective-permute-start.6 = (bf16[4,16,64,128]{3,2,1,0:T(8,128)(2,1)S(1)}, bf16[4,16,64,128]{3,2,1,0:T(8,128)(2,1)S(1)}, u32[]{:S(2)}, u32[]{:S(2)}) collective-permute-start(bf16[4,16,64,128]{3,2,1,0:T(8,128)(2,1)S(1)} %collective-permute-done.refs_2_), channel_id=1, source_target_pairs={{0,1},{1,0},{2,3},{3,2},{4,5},{5,4},{6,7},{7,6},{8,9},{9,8},{10,11... | collective-permute-start | bytes 3145736 | tf_op jit(solution)/shard_map/ppermute | solution.py:193
  88.8 3.2 %collective-permute-start.7 = (bf16[4,8,64,128]{3,2,1,0:T(8,128)(2,1)S(1)}, bf16[4,8,64,128]{3,2,1,0:T(8,128)(2,1)S(1)}, u32[]{:S(2)}, u32[]{:S(2)}) collective-permute-start(bf16[4,8,64,128]{3,2,1,0:T(8,128)(2,1)S(1)} %collective-permute-done.3.refs_3_), channel_id=1, source_target_pairs={{0,1},{1,0},{2,3},{3,2},{4,5},{5,4},{6,7},{7,6},{8,9},{9,8},{10,11... | collective-permute-start | bytes 1572872 | tf_op jit(solution)/shard_map/ppermute | solution.py:193
  92.0 1.9 %collective-permute-start.8 = (bf16[4,8,64,128]{3,2,1,0:T(8,128)(2,1)S(1)}, bf16[4,8,64,128]{3,2,1,0:T(8,128)(2,1)S(1)}, u32[]{:S(2)}, u32[]{:S(2)}) collective-permute-start(bf16[4,8,64,128]{3,2,1,0:T(8,128)(2,1)S(1)} %collective-permute-done.4.refs_4_), channel_id=1, source_target_pairs={{0,1},{1,0},{2,3},{3,2},{4,5},{5,4},{6,7},{7,6},{8,9},{9,8},{10,11... | collective-permute-start | bytes 1572872 | tf_op jit(solution)/shard_map/ppermute | solution.py:193
  94.0 1.9 %collective-permute-done.8.refs_9_ = bf16[4,8,64,128]{3,2,1,0:T(8,128)(2,1)S(1)} collective-permute-done((bf16[4,8,64,128]{3,2,1,0:T(8,128)(2,1)S(1)}, bf16[4,8,64,128]{3,2,1,0:T(8,128)(2,1)S(1)}, u32[]{:S(2)}, u32[]{:S(2)}) %collective-permute-start.8) | collective-permute-done | bytes 524320 | tf_op jit(solution)/shard_map/ppermute | solution.py:193
  95.8 5.0 %project.1 = bf16[384,2048]{1,0:T(8,128)(2,1)} custom-call(bf16[384,2048]{1,0:T(8,128)(2,1)S(1)} %copy-done.5, bf16[4,16,64,128]{3,2,1,0:T(8,128)(2,1)S(1)} %all-to-all-done.1.refs_0_, bf16[4,16,64,128]{3,2,1,0:T(8,128)(2,1)S(1)} %collective-permute-done.1.refs_1_, bf16[4,16,64,128]{3,2,1,0:T(8,128)(2,1)S(1)} %collective-permute-done.refs_2_, ...), custom_call_target="tpu_custom_call" | custom-call | flops 3221225472 | bytes 12582912 | tf_op jit(solution)/shard_map/project/pallas_call | solution.py:134
  (24 shorter events, 2.0 us)
Async XLA Ops:
  1.5 29.5 %all-to-all-start = ((bf16[16,64,128]{2,1,0:T(8,128)(2,1)}), bf16[16,64,128]{2,1,0:T(8,128)(2,1)S(1)}, u32[]{:S(2)}, u32[]{:S(2)}) async-start(bf16[16,64,128]{2,1,0:T(8,128)(2,1)} %broadcast_in_dim.8), calls=%async_computation | async-start | bytes 524288 | tf_op jit(solution)/shard_map/all_to_all | solution.py:169
  17.2 1.4 %copy-start = (bf16[1,384,2048]{2,1,0:T(8,128)(2,1)S(1)}, bf16[1,384,2048]{2,1,0:T(8,128)(2,1)}, u32[]{:S(2)}) copy-start(bf16[1,384,2048]{2,1,0:T(8,128)(2,1)} %param.7) | copy-start | bytes 4718596
  18.6 0.7 copy-start.3
  22.4 1.1 %copy-start.6 = (bf16[384,2048]{1,0:T(8,128)(2,1)}, bf16[384,2048]{1,0:T(8,128)(2,1)S(1)}, u32[]{:S(2)}) copy-start(bf16[384,2048]{1,0:T(8,128)(2,1)S(1)} %norm.1.normed_ref) | copy-start | bytes 4718596
  23.5 12.7 %copy-start.8 = (f32[16,128]{1,0:T(8,128)S(1)}, f32[16,128]{1,0:T(8,128)}, u32[]{:S(2)}) copy-start(f32[16,128]{1,0:T(8,128)} %param.10) | copy-start | bytes 24580
  23.5 12.8 %copy-start.1 = (bf16[1,384,2048]{2,1,0:T(8,128)(2,1)S(1)}, bf16[1,384,2048]{2,1,0:T(8,128)(2,1)}, u32[]{:S(2)}) copy-start(bf16[1,384,2048]{2,1,0:T(8,128)(2,1)} %param.6) | copy-start | bytes 4718596
  23.5 12.8 %copy-start.2 = (bf16[16,128,128]{2,1,0:T(8,128)(2,1)S(1)}, bf16[16,128,128]{2,1,0:T(8,128)(2,1)}, u32[]{:S(2)}) copy-start(bf16[16,128,128]{2,1,0:T(8,128)(2,1)} %weight_ref.1) | copy-start | bytes 1572868
  32.2 13.8 %all-to-all-start.1 = ((bf16[4,16,64,128]{3,2,1,0:T(8,128)(2,1)}), bf16[4,16,64,128]{3,2,1,0:T(8,128)(2,1)S(1)}, u32[]{:S(2)}, u32[]{:S(2)}) async-start(bf16[4,16,64,128]{3,2,1,0:T(8,128)(2,1)} %broadcast_in_dim.20), calls=%async_computation.1 | async-start | bytes 2097152 | tf_op jit(solution)/shard_map/all_to_all | solution.py:169
  36.4 1.4 %copy-start.7 = (bf16[384,2048]{1,0:T(8,128)(2,1)S(1)}, bf16[384,2048]{1,0:T(8,128)(2,1)}, u32[]{:S(2)}) copy-start(bf16[384,2048]{1,0:T(8,128)(2,1)} %copy-done.6) | copy-start | bytes 4718596
  39.3 1.1 %copy-start.4 = (bf16[384,2048]{1,0:T(8,128)(2,1)}, bf16[384,2048]{1,0:T(8,128)(2,1)S(1)}, u32[]{:S(2)}) copy-start(bf16[384,2048]{1,0:T(8,128)(2,1)S(1)} %gate.1.gated_ref) | copy-start | bytes 4718596
  46.0 49.8 %copy-start.5 = (bf16[384,2048]{1,0:T(8,128)(2,1)S(1)}, bf16[384,2048]{1,0:T(8,128)(2,1)}, u32[]{:S(2)}) copy-start(bf16[384,2048]{1,0:T(8,128)(2,1)} %copy-done.4) | copy-start | bytes 4718596
  46.0 14.5 %collective-permute-start.2 = (bf16[4,16,64,128]{3,2,1,0:T(8,128)(2,1)S(1)}, bf16[4,16,64,128]{3,2,1,0:T(8,128)(2,1)S(1)}, u32[]{:S(2)}, u32[]{:S(2)}) collective-permute-start(bf16[4,16,64,128]{3,2,1,0:T(8,128)(2,1)S(1)} %all-to-all-done.1.refs_0_), channel_id=1, source_target_pairs={{0,1},{1,0},{2,3},{3,2},{4,5},{5,4},{6,7},{7,6},{8,9},{9,8},{10,11... | collective-permute-start | bytes 3145736 | tf_op jit(solution)/shard_map/ppermute | solution.py:188
  55.2 15.8 %collective-permute-start.1 = (bf16[4,16,64,128]{3,2,1,0:T(8,128)(2,1)S(1)}, bf16[4,16,64,128]{3,2,1,0:T(8,128)(2,1)S(1)}, u32[]{:S(2)}, u32[]{:S(2)}) collective-permute-start(bf16[4,16,64,128]{3,2,1,0:T(8,128)(2,1)S(1)} %all-to-all-done.1.refs_0_), channel_id=1, source_target_pairs={{0,6},{1,25},{2,0},{3,27},{4,2},{5,29},{6,4},{7,31},{8,14},{9,1},{... | collective-permute-start | bytes 3145736 | tf_op jit(solution)/shard_map/ppermute | solution.py:187
  58.0 17.0 %collective-permute-start = (bf16[4,16,64,128]{3,2,1,0:T(8,128)(2,1)S(1)}, bf16[4,16,64,128]{3,2,1,0:T(8,128)(2,1)S(1)}, u32[]{:S(2)}, u32[]{:S(2)}) collective-permute-start(bf16[4,16,64,128]{3,2,1,0:T(8,128)(2,1)S(1)} %all-to-all-done.1.refs_0_), channel_id=1, source_target_pairs={{0,2},{1,9},{2,4},{3,11},{4,6},{5,13},{6,0},{7,15},{8,10},{9,17},{... | collective-permute-start | bytes 3145736 | tf_op jit(solution)/shard_map/ppermute | solution.py:186
  75.1 13.7 %collective-permute-start.3 = (bf16[4,8,64,128]{3,2,1,0:T(8,128)(2,1)S(1)}, bf16[4,8,64,128]{3,2,1,0:T(8,128)(2,1)S(1)}, u32[]{:S(2)}, u32[]{:S(2)}) collective-permute-start(bf16[4,8,64,128]{3,2,1,0:T(8,128)(2,1)S(1)} %slice.6), channel_id=1, source_target_pairs={{0,2},{1,9},{2,4},{3,11},{4,6},{5,13},{6,0},{7,15},{8,10},{9,17},{... | collective-permute-start | bytes 1572872 | tf_op jit(solution)/shard_map/ppermute | solution.py:190
  77.0 15.0 %collective-permute-start.4 = (bf16[4,8,64,128]{3,2,1,0:T(8,128)(2,1)S(1)}, bf16[4,8,64,128]{3,2,1,0:T(8,128)(2,1)S(1)}, u32[]{:S(2)}, u32[]{:S(2)}) collective-permute-start(bf16[4,8,64,128]{3,2,1,0:T(8,128)(2,1)S(1)} %slice.7), channel_id=1, source_target_pairs={{0,6},{1,25},{2,0},{3,27},{4,2},{5,29},{6,4},{7,31},{8,14},{9,1},{... | collective-permute-start | bytes 1572872 | tf_op jit(solution)/shard_map/ppermute | solution.py:191
  81.6 14.2 %collective-permute-start.5 = (bf16[4,16,64,128]{3,2,1,0:T(8,128)(2,1)S(1)}, bf16[4,16,64,128]{3,2,1,0:T(8,128)(2,1)S(1)}, u32[]{:S(2)}, u32[]{:S(2)}) collective-permute-start(bf16[4,16,64,128]{3,2,1,0:T(8,128)(2,1)S(1)} %collective-permute-done.1.refs_1_), channel_id=1, source_target_pairs={{0,1},{1,0},{2,3},{3,2},{4,5},{5,4},{6,7},{7,6},{8,9},{9,8},{10,11... | collective-permute-start | bytes 3145736 | tf_op jit(solution)/shard_map/ppermute | solution.py:193
  86.8 9.0 %collective-permute-start.6 = (bf16[4,16,64,128]{3,2,1,0:T(8,128)(2,1)S(1)}, bf16[4,16,64,128]{3,2,1,0:T(8,128)(2,1)S(1)}, u32[]{:S(2)}, u32[]{:S(2)}) collective-permute-start(bf16[4,16,64,128]{3,2,1,0:T(8,128)(2,1)S(1)} %collective-permute-done.refs_2_), channel_id=1, source_target_pairs={{0,1},{1,0},{2,3},{3,2},{4,5},{5,4},{6,7},{7,6},{8,9},{9,8},{10,11... | collective-permute-start | bytes 3145736 | tf_op jit(solution)/shard_map/ppermute | solution.py:193
  88.8 5.2 %collective-permute-start.7 = (bf16[4,8,64,128]{3,2,1,0:T(8,128)(2,1)S(1)}, bf16[4,8,64,128]{3,2,1,0:T(8,128)(2,1)S(1)}, u32[]{:S(2)}, u32[]{:S(2)}) collective-permute-start(bf16[4,8,64,128]{3,2,1,0:T(8,128)(2,1)S(1)} %collective-permute-done.3.refs_3_), channel_id=1, source_target_pairs={{0,1},{1,0},{2,3},{3,2},{4,5},{5,4},{6,7},{7,6},{8,9},{9,8},{10,11... | collective-permute-start | bytes 1572872 | tf_op jit(solution)/shard_map/ppermute | solution.py:193
  92.0 3.8 %collective-permute-start.8 = (bf16[4,8,64,128]{3,2,1,0:T(8,128)(2,1)S(1)}, bf16[4,8,64,128]{3,2,1,0:T(8,128)(2,1)S(1)}, u32[]{:S(2)}, u32[]{:S(2)}) collective-permute-start(bf16[4,8,64,128]{3,2,1,0:T(8,128)(2,1)S(1)} %collective-permute-done.4.refs_4_), channel_id=1, source_target_pairs={{0,1},{1,0},{2,3},{3,2},{4,5},{5,4},{6,7},{7,6},{8,9},{9,8},{10,11... | collective-permute-start | bytes 1572872 | tf_op jit(solution)/shard_map/ppermute | solution.py:193

commit v2 on v1

--- a/solution.py
+++ b/solution.py
@@ -1,11 +1,10 @@
-import functools
-
 import jax
 import jax.numpy as jnp
 from jax import lax
 from jax.experimental import pallas as pl
 from jax.experimental.pallas import tpu as pltpu
 from jax.sharding import PartitionSpec as P
+
 
 BLOCK = 128
 norm_epsilon = 1e-05
@@ -62,16 +61,17 @@
     keep = lax.broadcasted_iota(jnp.int32, (block, block), 0) >= lax.broadcasted_iota(
         jnp.int32, (block, block), 1
     )
+    bias = jnp.transpose(bias_ref[...])
     for g in range(groups):
         cols = slice(g * width, (g + 1) * width)
         masked = jnp.where(keep, weight_ref[g].astype(F32), 0.0).astype(BF)
         mixed = jnp.dot(masked, normed_ref[:, cols], preferred_element_type=F32)
-        mixed = mixed + bias_ref[:, g : g + 1]
+        mixed = mixed + bias[:, g : g + 1]
         up = gelu(up_ref[:, cols].astype(F32)).astype(BF).astype(F32)
         out_ref[:, cols] = (up * mixed).astype(BF)
 
 
-def gate(normed, up, weight, bias_t):
+def gate(normed, up, weight, bias):
     rows, width = up.shape
     groups = weight.shape[0]
     return pl.pallas_call(
@@ -81,7 +81,7 @@
             pl.BlockSpec((BLOCK, width), lambda i: (i, 0)),
             pl.BlockSpec((BLOCK, width), lambda i: (i, 0)),
             pl.BlockSpec((groups, BLOCK, BLOCK), lambda i: (0, 0, 0)),
-            pl.BlockSpec((BLOCK, groups), lambda i: (0, 0)),
+            pl.BlockSpec((groups, BLOCK), lambda i: (0, 0)),
         ],
         out_specs=pl.BlockSpec((BLOCK, width), lambda i: (i, 0)),
         out_shape=jax.ShapeDtypeStruct((rows, width), BF),
@@ -90,22 +90,32 @@
             flops=4_000_000_000, bytes_accessed=rows * width * 6, transcendentals=rows * width
         ),
         name="gate",
-    )(normed, up, weight, bias_t)
+    )(normed, up, weight, bias)
 
 
 def project_kernel(gated_ref, *refs):
-    own, other, out_ref = refs[:5], refs[5:10], refs[10]
+    pieces, out_ref = refs[:-1], refs[-1]
     index = lax.axis_index("dp")
     core, x, y = index & 1, (index >> 1) & 3, index >> 3
     first, second = lax.select(core == 0, x, y), lax.select(core == 0, y, x)
-    blocks = own[0].shape[1]
+    own, low1, high1, low2, high2, low3, high3, other, near, far = pieces
+    blocks = own.shape[1]
     half = blocks // 2
-    pair = 2 * own[0].shape[2]
-
-    def tile(refs, r, j, k):
+    pair = 2 * own.shape[2]
+
+    def mine(r, j, k):
+        if r == 0:
+            return own[j, k]
+        low, high = ((low1, high1), (low2, high2), (low3, high3))[r - 1]
+        return low[j, k] if k < half else high[j, k - half]
+
+    def theirs(r, j, k):
+        if r == 0:
+            return other[j, k]
+        part = k // half
         if r == 2:
-            return refs[3][j, k] if k < half else refs[4][j, k - half]
-        return refs[(0, 1, None, 2)[r]][j, k]
+            return far[part, j, k % half]
+        return near[(r - 1) + part, j, k % half]
 
     for r in range(4):
         a = lax.rem(first + r, 4)
@@ -115,8 +125,8 @@
             for t in (s, s + 1):
                 b = lax.rem(second + t, 4)
                 at.append(lax.select(core == 0, b * 4 + a, a * 4 + b))
-                rhs.append([tile(own, r, b, k) for k in range(blocks)])
-                rhs.append([tile(other, t, a, k) for k in range(blocks)])
+                rhs.append([mine(r, b, k) for k in range(blocks)])
+                rhs.append([theirs(t, a, k) for k in range(blocks)])
             whole = jnp.concatenate([jnp.concatenate(x, axis=1) for x in rhs], axis=0)
             result = lax.dot_general(
                 gated_ref[...], whole, (((1,), (1,)), ((), ())), preferred_element_type=F32
@@ -127,13 +137,13 @@
                 out_ref[:, where] = part.astype(BF)
 
 
-def project(gated, own, other):
+def project(gated, pieces):
     rows = gated.shape[0]
-    width = 16 * 2 * own[0].shape[2]
+    width = 16 * 2 * pieces[0].shape[2]
     vmem = pl.BlockSpec(memory_space=pltpu.VMEM)
     return pl.pallas_call(
         project_kernel,
-        in_specs=[vmem] * 11,
+        in_specs=[vmem] * (1 + len(pieces)),
         out_specs=vmem,
         out_shape=jax.ShapeDtypeStruct((rows, width), BF),
         compiler_params=pltpu.CompilerParams(vmem_limit_bytes=6 << 20),
@@ -141,7 +151,7 @@
             flops=2 * rows * width * gated.shape[1], bytes_accessed=12 << 20, transcendentals=0
         ),
         name="project",
-    )(gated, *own, *other)
+    )(gated, *pieces)
 
 
 def at(y, x, core):
@@ -176,22 +186,30 @@
     )
 
 
+def moved(value, pairs):
+    return lax.ppermute(value, "dp", pairs)
+
+
 def per_device(up_pre, mix_pre, ln_gain, mix_weight, mix_bias, out_weight):
     slab = sent_to_all(out_weight.T, "sp", 16)
+    own = sent_to_all(slab, "dp", 4, GROUPS)
+    low, high = own[:, :8], own[:, 8:]
+    low3 = moved(low, ring(1))
+    high1 = moved(high, ring(-1))
+    high3 = moved(high, ring(1))
+    low1 = moved(low, ring(-1))
+    low3, high1, ln_gain = lax.optimization_barrier((low3, high1, ln_gain))
+    low2 = moved(low3, ring(1))
+    high2 = moved(high1, ring(-1))
+    other = moved(own, SWAP)
     normed = norm(mix_pre[0], ln_gain[None])
-    slab, normed = lax.optimization_barrier((slab, normed))
-    own = sent_to_all(slab, "dp", 4, GROUPS)
-    gated = gate(normed, up_pre[0], mix_weight, mix_bias.T)
-    own, gated = lax.optimization_barrier((own, gated))
-    before = lax.ppermute(own, "dp", ring(1))
-    after = lax.ppermute(own, "dp", ring(-1))
-    other = lax.ppermute(own, "dp", SWAP)
-    before, after, other = lax.optimization_barrier((before, after, other))
-    far_low = lax.ppermute(before[:, :8], "dp", ring(1))
-    far_high = lax.ppermute(after[:, 8:], "dp", ring(-1))
-    mine = [own, after, before, far_low, far_high]
-    theirs = [other] + [lax.ppermute(v, "dp", SWAP) for v in mine[1:]]
-    return project(gated, mine, theirs)[None]
+    low1, high3, normed = lax.optimization_barrier((low1, high3, normed))
+    near = moved(jnp.stack([low1, high1, low3, high3]), SWAP)
+    gated = gate(normed, up_pre[0], mix_weight, mix_bias)
+    low2, high2, gated = lax.optimization_barrier((low2, high2, gated))
+    far = moved(jnp.stack([low2, high2]), SWAP)
+    pieces = [own, low1, high1, low2, high2, low3, high3, other, near, far]
+    return project(gated, pieces)[None]
 
 
 def solution(mesh):

time: 101 us -> 101 us (level)
  blocking collectives: 0 us -> 43 us
  waiting for transfers between devices: 29.4 us -> 10.2 us
  starting transfers between devices: 53 us -> 36 us
  local copies, waits for them, and re-layouts: 8.67 us -> 1.1 us
    all_to_all x0 -> x2, blocking collectives: none -> 43 us  [sent_to_all(): lax.all_to_all(jnp.broadcast_to(value[None], (length, *value.shape)), axi...]
    all_to_all x2 -> x0, starting transfers between devices: 19.7 us -> none  [sent_to_all(): lax.all_to_all(jnp.broadcast_to(value[None], (length, *value.shape)), axi...]
    all_to_all x2 -> x0, waiting for transfers between devices: 13 us -> none  [sent_to_all(): lax.all_to_all(jnp.broadcast_to(value[None], (length, *value.shape)), axi...]
    ppermute x9, waiting for transfers between devices: 16.4 us -> 10.2 us  [moved(): return lax.ppermute(value, 'dp', pairs)]
    unnamed x19 -> x10, local copies, waits for them, and re-layouts: 5.89 us -> 0.02 us
    ppermute x9, starting transfers between devices: 33.2 us -> 36 us  [moved(): return lax.ppermute(value, 'dp', pairs)]
    broadcast_in_dim x2, local copies, waits for them, and re-layouts: 2.71 us -> 1 us  [sent_to_all(): jnp.broadcast_to(value[None], (length, *value.shape))]
  transfers between devices with their start and end apart: 11 -> 9, of which waited for: 5 -> 6; matrix products, arithmetic and copies ran while one was open for 0% -> 0% of each run, Pallas kernels for 5% -> 5%
where the time goes in v2:
time: 101 us
  blocking collectives  43 us (43%)
  starting transfers between devices  36 us (36%)
  waiting for transfers between devices  10.2 us (10%)
  Pallas kernels  9.75 us (10%)
  local copies, waits for them, and re-layouts  1.1 us (1%)
    all_to_all x2, blocking collectives, sent_to_all(): lax.all_to_all(jnp.broadcast_to(value[None], (length, *value.shape)), axi...  43 us
    ppermute x9, starting transfers between devices, moved(): return lax.ppermute(value, 'dp', pairs)  36 us
    ppermute x9, waiting for transfers between devices, moved(): return lax.ppermute(value, 'dp', pairs)  10.2 us
    pallas_call x1, Pallas kernels, project(): pl.pallas_call(project_kernel, in_specs=[vmem] * (1 + len(pieces)), out_s...  4.98 us
    pallas_call x1, Pallas kernels, norm(): pl.pallas_call(norm_kernel, grid=(rows // BLOCK,), in_specs=[pl.BlockSpec...  3.06 us
  transfers between devices with their start and end apart: 9, of which 6 were waited for; matrix products, arithmetic and copies ran while one was open for 0% of the time, Pallas kernels for 5%

profile of v2, /device:TPU:1, one launch (start us, length us, event | category | flops | bytes accessed | tf_op | source)
XLA Modules:
  0.0 100.7 jit_solution(17799505506483622784)
XLA Ops:
  0.0 0.8 broadcast_in_dim.8
  0.8 29.3 %all_to_all.10 = bf16[16,64,128]{2,1,0:T(8,128)(2,1)S(1)} all-to-all(bf16[16,64,128]{2,1,0:T(8,128)(2,1)S(1)} %broadcast_in_dim.8), channel_id=1, replica_groups=mesh['sp'=16,'dp'=32] {'sp'}, dimensions={0} | all-to-all | bytes 524288 | tf_op jit(solution)/shard_map/all_to_all | solution.py:179
  30.1 0.2 broadcast_in_dim.9
  30.4 13.7 %all_to_all.11.refs_0_ = bf16[4,16,64,128]{3,2,1,0:T(8,128)(2,1)S(1)} all-to-all(bf16[4,16,64,128]{3,2,1,0:T(8,128)(2,1)S(1)} %broadcast_in_dim.9), channel_id=1, replica_groups={{0,8,16,24},{2,10,18,26},{4,12,20,28},{6,14,22,30},{1,3,5,7},{9,11,13,1..., dimensions={0} | all-to-all | bytes 2097152 | tf_op jit(solution)/shard_map/all_to_all | solution.py:179
  44.1 3.2 %collective-permute-start = (bf16[4,8,64,128]{3,2,1,0:T(8,128)(2,1)S(1)}, bf16[4,8,64,128]{3,2,1,0:T(8,128)(2,1)S(1)}, u32[]{:S(2)}, u32[]{:S(2)}) collective-permute-start(bf16[4,8,64,128]{3,2,1,0:T(8,128)(2,1)S(1)} %get-tuple-element.24), channel_id=1, source_target_pairs={{0,2},{1,9},{2,4},{3,11},{4,6},{5,13},{6,0},{7,15},{8,10},{9,17},{... | collective-permute-start | bytes 1572872 | tf_op jit(solution)/shard_map/ppermute | solution.py:190
  47.3 3.4 %collective-permute-start.1 = (bf16[4,8,64,128]{3,2,1,0:T(8,128)(2,1)S(1)}, bf16[4,8,64,128]{3,2,1,0:T(8,128)(2,1)S(1)}, u32[]{:S(2)}, u32[]{:S(2)}) collective-permute-start(bf16[4,8,64,128]{3,2,1,0:T(8,128)(2,1)S(1)} %get-tuple-element.23), channel_id=1, source_target_pairs={{0,6},{1,25},{2,0},{3,27},{4,2},{5,29},{6,4},{7,31},{8,14},{9,1},{... | collective-permute-start | bytes 1572872 | tf_op jit(solution)/shard_map/ppermute | solution.py:190
  50.7 3.4 %collective-permute-start.4 = (bf16[4,8,64,128]{3,2,1,0:T(8,128)(2,1)S(1)}, bf16[4,8,64,128]{3,2,1,0:T(8,128)(2,1)S(1)}, u32[]{:S(2)}, u32[]{:S(2)}) collective-permute-start(bf16[4,8,64,128]{3,2,1,0:T(8,128)(2,1)S(1)} %get-tuple-element.24), channel_id=1, source_target_pairs={{0,6},{1,25},{2,0},{3,27},{4,2},{5,29},{6,4},{7,31},{8,14},{9,1},{... | collective-permute-start | bytes 1572872 | tf_op jit(solution)/shard_map/ppermute | solution.py:190
  54.1 1.9 %collective-permute-start.5 = (bf16[4,8,64,128]{3,2,1,0:T(8,128)(2,1)S(1)}, bf16[4,8,64,128]{3,2,1,0:T(8,128)(2,1)S(1)}, u32[]{:S(2)}, u32[]{:S(2)}) collective-permute-start(bf16[4,8,64,128]{3,2,1,0:T(8,128)(2,1)S(1)} %get-tuple-element.23), channel_id=1, source_target_pairs={{0,2},{1,9},{2,4},{3,11},{4,6},{5,13},{6,0},{7,15},{8,10},{9,17},{... | collective-permute-start | bytes 1572872 | tf_op jit(solution)/shard_map/ppermute | solution.py:190
  56.0 1.2 %collective-permute-done.1.refs_2_ = bf16[4,8,64,128]{3,2,1,0:T(8,128)(2,1)S(1)} collective-permute-done((bf16[4,8,64,128]{3,2,1,0:T(8,128)(2,1)S(1)}, bf16[4,8,64,128]{3,2,1,0:T(8,128)(2,1)S(1)}, u32[]{:S(2)}, u32[]{:S(2)}) %collective-permute-start.1) | collective-permute-done | bytes 524320 | tf_op jit(solution)/shard_map/ppermute | solution.py:190
  57.3 3.1 %norm.1.normed_ref = bf16[384,2048]{1,0:T(8,128)(2,1)S(1)} custom-call(bf16[384,2048]{1,0:T(8,128)(2,1)S(1)} %bitcast.17, f32[1,2048]{1,0:T(1,128)S(1)} %bitcast.19), custom_call_target="tpu_custom_call" | custom-call | flops 4000000000 | bytes 3145728 | tf_op jit(solution)/shard_map/norm/pallas_call | solution.py:40
  60.3 2.8 %collective-permute-done.4.refs_1_ = bf16[4,8,64,128]{3,2,1,0:T(8,128)(2,1)S(1)} collective-permute-done((bf16[4,8,64,128]{3,2,1,0:T(8,128)(2,1)S(1)}, bf16[4,8,64,128]{3,2,1,0:T(8,128)(2,1)S(1)}, u32[]{:S(2)}, u32[]{:S(2)}) %collective-permute-start.4) | collective-permute-done | bytes 524320 | tf_op jit(solution)/shard_map/ppermute | solution.py:190
  63.2 2.0 %collective-permute-done.5.refs_6_ = bf16[4,8,64,128]{3,2,1,0:T(8,128)(2,1)S(1)} collective-permute-done((bf16[4,8,64,128]{3,2,1,0:T(8,128)(2,1)S(1)}, bf16[4,8,64,128]{3,2,1,0:T(8,128)(2,1)S(1)}, u32[]{:S(2)}, u32[]{:S(2)}) %collective-permute-start.5) | collective-permute-done | bytes 524320 | tf_op jit(solution)/shard_map/ppermute | solution.py:190
  65.2 0.3 pad_maximum_fusion
  65.5 12.2 %collective-permute-start.7 = (bf16[4,4,8,64,128]{4,3,2,1,0:T(8,128)(2,1)S(1)}, bf16[4,4,8,64,128]{4,3,2,1,0:T(8,128)(2,1)S(1)}, u32[]{:S(2)}, u32[]{:S(2)}) collective-permute-start(bf16[4,4,8,64,128]{4,3,2,1,0:T(8,128)(2,1)S(1)} %pad_maximum_fusion), channel_id=1, source_target_pairs={{0,1},{1,0},{2,3},{3,2},{4,5},{5,4},{6,7},{7,6},{8,9},{9,8},{10,11... | collective-permute-start | bytes 6291464 | tf_op jit(solution)/shard_map/ppermute | solution.py:190
  77.6 1.9 %collective-permute-start.2 = (bf16[4,8,64,128]{3,2,1,0:T(8,128)(2,1)S(1)}, bf16[4,8,64,128]{3,2,1,0:T(8,128)(2,1)S(1)}, u32[]{:S(2)}, u32[]{:S(2)}) collective-permute-start(bf16[4,8,64,128]{3,2,1,0:T(8,128)(2,1)S(1)} %collective-permute-done.refs_5_), channel_id=1, source_target_pairs={{0,2},{1,9},{2,4},{3,11},{4,6},{5,13},{6,0},{7,15},{8,10},{9,17},{... | collective-permute-start | bytes 1572872 | tf_op jit(solution)/shard_map/ppermute | solution.py:190
  79.6 4.6 %collective-permute-start.3 = (bf16[4,8,64,128]{3,2,1,0:T(8,128)(2,1)S(1)}, bf16[4,8,64,128]{3,2,1,0:T(8,128)(2,1)S(1)}, u32[]{:S(2)}, u32[]{:S(2)}) collective-permute-start(bf16[4,8,64,128]{3,2,1,0:T(8,128)(2,1)S(1)} %collective-permute-done.1.refs_2_), channel_id=1, source_target_pairs={{0,6},{1,25},{2,0},{3,27},{4,2},{5,29},{6,4},{7,31},{8,14},{9,1},{... | collective-permute-start | bytes 1572872 | tf_op jit(solution)/shard_map/ppermute | solution.py:190
  84.2 2.5 %collective-permute-start.6 = (bf16[4,16,64,128]{3,2,1,0:T(8,128)(2,1)S(1)}, bf16[4,16,64,128]{3,2,1,0:T(8,128)(2,1)S(1)}, u32[]{:S(2)}, u32[]{:S(2)}) collective-permute-start(bf16[4,16,64,128]{3,2,1,0:T(8,128)(2,1)S(1)} %all_to_all.11.refs_0_), channel_id=1, source_target_pairs={{0,1},{1,0},{2,3},{3,2},{4,5},{5,4},{6,7},{7,6},{8,9},{9,8},{10,11... | collective-permute-start | bytes 3145736 | tf_op jit(solution)/shard_map/ppermute | solution.py:190
  86.7 1.7 %gate.1.gated_ref = bf16[384,2048]{1,0:T(8,128)(2,1)S(1)} custom-call(bf16[384,2048]{1,0:T(8,128)(2,1)S(1)} %norm.1.normed_ref, bf16[384,2048]{1,0:T(8,128)(2,1)S(1)} %bitcast.18, bf16[16,128,128]{2,1,0:T(8,128)(2,1)S(1)} %copy-done.2, f32[16,128]{1,0:T(8,128)S(1)} %copy-done.4), custom_call_target="tpu_custom_call" | custom-call | flops 4000000000 | bytes 4718592 | tf_op jit(solution)/shard_map/gate/pallas_call | solution.py:77
  88.4 0.7 collective-permute-done.2.refs_3_
  89.1 1.2 %collective-permute-done.3.refs_4_ = bf16[4,8,64,128]{3,2,1,0:T(8,128)(2,1)S(1)} collective-permute-done((bf16[4,8,64,128]{3,2,1,0:T(8,128)(2,1)S(1)}, bf16[4,8,64,128]{3,2,1,0:T(8,128)(2,1)S(1)}, u32[]{:S(2)}, u32[]{:S(2)}) %collective-permute-start.3) | collective-permute-done | bytes 524320 | tf_op jit(solution)/shard_map/ppermute | solution.py:190
  90.3 0.1 pad_maximum_fusion.1
  90.4 3.1 %collective-permute-start.8 = (bf16[2,4,8,64,128]{4,3,2,1,0:T(8,128)(2,1)S(1)}, bf16[2,4,8,64,128]{4,3,2,1,0:T(8,128)(2,1)S(1)}, u32[]{:S(2)}, u32[]{:S(2)}) collective-permute-start(bf16[2,4,8,64,128]{4,3,2,1,0:T(8,128)(2,1)S(1)} %pad_maximum_fusion.1), channel_id=1, source_target_pairs={{0,1},{1,0},{2,3},{3,2},{4,5},{5,4},{6,7},{7,6},{8,9},{9,8},{10,11... | collective-permute-start | bytes 3145736 | tf_op jit(solution)/shard_map/ppermute | solution.py:190
  93.4 2.3 %collective-permute-done.8.refs_9_ = bf16[2,4,8,64,128]{4,3,2,1,0:T(8,128)(2,1)S(1)} collective-permute-done((bf16[2,4,8,64,128]{4,3,2,1,0:T(8,128)(2,1)S(1)}, bf16[2,4,8,64,128]{4,3,2,1,0:T(8,128)(2,1)S(1)}, u32[]{:S(2)}, u32[]{:S(2)}) %collective-permute-start.8) | collective-permute-done | bytes 1048608 | tf_op jit(solution)/shard_map/ppermute | solution.py:190
  95.7 5.0 %project.1 = bf16[384,2048]{1,0:T(8,128)(2,1)} custom-call(bf16[384,2048]{1,0:T(8,128)(2,1)S(1)} %gate.1.gated_ref, bf16[4,16,64,128]{3,2,1,0:T(8,128)(2,1)S(1)} %all_to_all.11.refs_0_, bf16[4,8,64,128]{3,2,1,0:T(8,128)(2,1)S(1)} %collective-permute-done.4.refs_1_, bf16[4,8,64,128]{3,2,1,0:T(8,128)(2,1)S(1)} %collective-permute-done.1.refs_2_, ...), custom_call_target="tpu_custom_call" | custom-call | flops 3221225472 | bytes 12582912 | tf_op jit(solution)/shard_map/project/pallas_call | solution.py:144
  (14 shorter events, 0.1 us)
Async XLA Ops:
  30.3 26.9 %copy-start = (bf16[1,384,2048]{2,1,0:T(8,128)(2,1)S(1)}, bf16[1,384,2048]{2,1,0:T(8,128)(2,1)}, u32[]{:S(2)}) copy-start(bf16[1,384,2048]{2,1,0:T(8,128)(2,1)} %param.7) | copy-start | bytes 4718596
  30.3 26.9 %copy-start.3 = (f32[2048]{0:T(1024)S(1)}, f32[2048]{0:T(1024)}, u32[]{:S(2)}) copy-start(f32[2048]{0:T(1024)} %param.8) | copy-start | bytes 24580
  44.1 11.9 %collective-permute-start = (bf16[4,8,64,128]{3,2,1,0:T(8,128)(2,1)S(1)}, bf16[4,8,64,128]{3,2,1,0:T(8,128)(2,1)S(1)}, u32[]{:S(2)}, u32[]{:S(2)}) collective-permute-start(bf16[4,8,64,128]{3,2,1,0:T(8,128)(2,1)S(1)} %get-tuple-element.24), channel_id=1, source_target_pairs={{0,2},{1,9},{2,4},{3,11},{4,6},{5,13},{6,0},{7,15},{8,10},{9,17},{... | collective-permute-start | bytes 1572872 | tf_op jit(solution)/shard_map/ppermute | solution.py:190
  47.3 9.9 %collective-permute-start.1 = (bf16[4,8,64,128]{3,2,1,0:T(8,128)(2,1)S(1)}, bf16[4,8,64,128]{3,2,1,0:T(8,128)(2,1)S(1)}, u32[]{:S(2)}, u32[]{:S(2)}) collective-permute-start(bf16[4,8,64,128]{3,2,1,0:T(8,128)(2,1)S(1)} %get-tuple-element.23), channel_id=1, source_target_pairs={{0,6},{1,25},{2,0},{3,27},{4,2},{5,29},{6,4},{7,31},{8,14},{9,1},{... | collective-permute-start | bytes 1572872 | tf_op jit(solution)/shard_map/ppermute | solution.py:190
  50.7 12.5 %collective-permute-start.4 = (bf16[4,8,64,128]{3,2,1,0:T(8,128)(2,1)S(1)}, bf16[4,8,64,128]{3,2,1,0:T(8,128)(2,1)S(1)}, u32[]{:S(2)}, u32[]{:S(2)}) collective-permute-start(bf16[4,8,64,128]{3,2,1,0:T(8,128)(2,1)S(1)} %get-tuple-element.24), channel_id=1, source_target_pairs={{0,6},{1,25},{2,0},{3,27},{4,2},{5,29},{6,4},{7,31},{8,14},{9,1},{... | collective-permute-start | bytes 1572872 | tf_op jit(solution)/shard_map/ppermute | solution.py:190
  54.1 11.1 %collective-permute-start.5 = (bf16[4,8,64,128]{3,2,1,0:T(8,128)(2,1)S(1)}, bf16[4,8,64,128]{3,2,1,0:T(8,128)(2,1)S(1)}, u32[]{:S(2)}, u32[]{:S(2)}) collective-permute-start(bf16[4,8,64,128]{3,2,1,0:T(8,128)(2,1)S(1)} %get-tuple-element.23), channel_id=1, source_target_pairs={{0,2},{1,9},{2,4},{3,11},{4,6},{5,13},{6,0},{7,15},{8,10},{9,17},{... | collective-permute-start | bytes 1572872 | tf_op jit(solution)/shard_map/ppermute | solution.py:190
  65.2 21.4 %copy-start.1 = (bf16[1,384,2048]{2,1,0:T(8,128)(2,1)S(1)}, bf16[1,384,2048]{2,1,0:T(8,128)(2,1)}, u32[]{:S(2)}) copy-start(bf16[1,384,2048]{2,1,0:T(8,128)(2,1)} %param.6) | copy-start | bytes 4718596
  65.2 21.4 %copy-start.2 = (bf16[16,128,128]{2,1,0:T(8,128)(2,1)S(1)}, bf16[16,128,128]{2,1,0:T(8,128)(2,1)}, u32[]{:S(2)}) copy-start(bf16[16,128,128]{2,1,0:T(8,128)(2,1)} %weight_ref.1) | copy-start | bytes 1572868
  65.2 21.5 %copy-start.4 = (f32[16,128]{1,0:T(8,128)S(1)}, f32[16,128]{1,0:T(8,128)}, u32[]{:S(2)}) copy-start(f32[16,128]{1,0:T(8,128)} %bias_ref.1) | copy-start | bytes 24580
  65.5 30.2 %collective-permute-start.7 = (bf16[4,4,8,64,128]{4,3,2,1,0:T(8,128)(2,1)S(1)}, bf16[4,4,8,64,128]{4,3,2,1,0:T(8,128)(2,1)S(1)}, u32[]{:S(2)}, u32[]{:S(2)}) collective-permute-start(bf16[4,4,8,64,128]{4,3,2,1,0:T(8,128)(2,1)S(1)} %pad_maximum_fusion), channel_id=1, source_target_pairs={{0,1},{1,0},{2,3},{3,2},{4,5},{5,4},{6,7},{7,6},{8,9},{9,8},{10,11... | collective-permute-start | bytes 6291464 | tf_op jit(solution)/shard_map/ppermute | solution.py:190
  77.6 11.4 %collective-permute-start.2 = (bf16[4,8,64,128]{3,2,1,0:T(8,128)(2,1)S(1)}, bf16[4,8,64,128]{3,2,1,0:T(8,128)(2,1)S(1)}, u32[]{:S(2)}, u32[]{:S(2)}) collective-permute-start(bf16[4,8,64,128]{3,2,1,0:T(8,128)(2,1)S(1)} %collective-permute-done.refs_5_), channel_id=1, source_target_pairs={{0,2},{1,9},{2,4},{3,11},{4,6},{5,13},{6,0},{7,15},{8,10},{9,17},{... | collective-permute-start | bytes 1572872 | tf_op jit(solution)/shard_map/ppermute | solution.py:190
  79.6 10.7 %collective-permute-start.3 = (bf16[4,8,64,128]{3,2,1,0:T(8,128)(2,1)S(1)}, bf16[4,8,64,128]{3,2,1,0:T(8,128)(2,1)S(1)}, u32[]{:S(2)}, u32[]{:S(2)}) collective-permute-start(bf16[4,8,64,128]{3,2,1,0:T(8,128)(2,1)S(1)} %collective-permute-done.1.refs_2_), channel_id=1, source_target_pairs={{0,6},{1,25},{2,0},{3,27},{4,2},{5,29},{6,4},{7,31},{8,14},{9,1},{... | collective-permute-start | bytes 1572872 | tf_op jit(solution)/shard_map/ppermute | solution.py:190
  84.2 9.3 %collective-permute-start.6 = (bf16[4,16,64,128]{3,2,1,0:T(8,128)(2,1)S(1)}, bf16[4,16,64,128]{3,2,1,0:T(8,128)(2,1)S(1)}, u32[]{:S(2)}, u32[]{:S(2)}) collective-permute-start(bf16[4,16,64,128]{3,2,1,0:T(8,128)(2,1)S(1)} %all_to_all.11.refs_0_), channel_id=1, source_target_pairs={{0,1},{1,0},{2,3},{3,2},{4,5},{5,4},{6,7},{7,6},{8,9},{9,8},{10,11... | collective-permute-start | bytes 3145736 | tf_op jit(solution)/shard_map/ppermute | solution.py:190
  90.4 5.3 %collective-permute-start.8 = (bf16[2,4,8,64,128]{4,3,2,1,0:T(8,128)(2,1)S(1)}, bf16[2,4,8,64,128]{4,3,2,1,0:T(8,128)(2,1)S(1)}, u32[]{:S(2)}, u32[]{:S(2)}) collective-permute-start(bf16[2,4,8,64,128]{4,3,2,1,0:T(8,128)(2,1)S(1)} %pad_maximum_fusion.1), channel_id=1, source_target_pairs={{0,1},{1,0},{2,3},{3,2},{4,5},{5,4},{6,7},{7,6},{8,9},{9,8},{10,11... | collective-permute-start | bytes 3145736 | tf_op jit(solution)/shard_map/ppermute | solution.py:190

commit v3 on v1

v3 whole, which is shorter than its diff:
```python
import jax
import jax.numpy as jnp
from jax import lax
from jax.experimental import pallas as pl
from jax.experimental.pallas import tpu as pltpu
from jax.sharding import PartitionSpec as P


BLOCK = 128
norm_epsilon = 1e-05
HALF_ROOT = 0.7071067811865476
BF = jnp.bfloat16
F32 = jnp.float32


def gelu(x):
    return (0.5 * x) * (1.0 + lax.erf(x * HALF_ROOT))


def norm_kernel(mix_ref, gain_ref, out_ref, act_ref):
    rows, width = mix_ref.shape
    step = 16

    def body(i, _):
        at = pl.ds(pl.multiple_of(i * step, step), step)
        act = gelu(mix_ref[at, :].astype(F32))
        act_ref[at, :] = act
        center = jnp.sum(act, axis=-1, keepdims=True) * (1.0 / width)
        off = act - center
        spread = jnp.sum(off * off, axis=-1, keepdims=True) * (1.0 / width)
        scale = lax.rsqrt(spread + norm_epsilon)
        out_ref[at, :] = ((act_ref[at, :] - center) * scale * gain_ref[...]).astype(BF)
        return 0

    lax.fori_loop(0, rows // step, body, 0, unroll=2)


def norm(mix, gain):
    rows, width = mix.shape
    return pl.pallas_call(
        norm_kernel,
        grid=(rows // BLOCK,),
        in_specs=[
            pl.BlockSpec((BLOCK, width), lambda i: (i, 0)),
            pl.BlockSpec((1, width), lambda i: (0, 0)),
        ],
        out_specs=pl.BlockSpec((BLOCK, width), lambda i: (i, 0)),
        out_shape=jax.ShapeDtypeStruct((rows, width), BF),
        scratch_shapes=[pltpu.VMEM((BLOCK, width), F32)],
        compiler_params=pltpu.CompilerParams(vmem_limit_bytes=8 << 20),
        cost_estimate=pl.CostEstimate(
            flops=4_000_000_000, bytes_accessed=rows * width * 4, transcendentals=rows * width
        ),
        name="norm",
    )(mix, gain)


def gate_kernel(normed_ref, up_ref, weight_ref, bias_ref, out_ref):
    groups, block, _ = weight_ref.shape
    width = up_ref.shape[1] // groups
    keep = lax.broadcasted_iota(jnp.int32, (block, block), 0) >= lax.broadcasted_iota(
        jnp.int32, (block, block), 1
    )
    bias = jnp.transpose(bias_ref[...])
    for g in range(groups):
        cols = slice(g * width, (g + 1) * width)
        masked = jnp.where(keep, weight_ref[g].astype(F32), 0.0).astype(BF)
        mixed = jnp.dot(masked, normed_ref[:, cols], preferred_element_type=F32)
        mixed = mixed + bias[:, g : g + 1]
        up = gelu(up_ref[:, cols].astype(F32)).astype(BF).astype(F32)
        out_ref[:, cols] = (up * mixed).astype(BF)


def gate(normed, up, weight, bias):
    rows, width = up.shape
    groups = weight.shape[0]
    return pl.pallas_call(
        gate_kernel,
        grid=(rows // BLOCK,),
        in_specs=[
            pl.BlockSpec((BLOCK, width), lambda i: (i, 0)),
            pl.BlockSpec((BLOCK, width), lambda i: (i, 0)),
            pl.BlockSpec((groups, BLOCK, BLOCK), lambda i: (0, 0, 0)),
            pl.BlockSpec((groups, BLOCK), lambda i: (0, 0)),
        ],
        out_specs=pl.BlockSpec((BLOCK, width), lambda i: (i, 0)),
        out_shape=jax.ShapeDtypeStruct((rows, width), BF),
        compiler_params=pltpu.CompilerParams(vmem_limit_bytes=8 << 20),
        cost_estimate=pl.CostEstimate(
            flops=4_000_000_000, bytes_accessed=rows * width * 6, transcendentals=rows * width
        ),
        name="gate",
    )(normed, up, weight, bias)


def project_kernel(mine_ref, partner_ref, *refs):
    pieces, kept_ref, sent_ref = refs[:-2], refs[-2], refs[-1]
    core = lax.axis_index("dp") & 1
    for n, piece in enumerate(pieces):
        count, blocks, width, _ = piece.shape
        rhs = jnp.concatenate(
            [
                jnp.concatenate([piece[j, k] for k in range(blocks)], axis=1)
                for j in range(count)
            ],
            axis=0,
        )
        for rows_ref, out_ref in ((mine_ref, kept_ref), (partner_ref, sent_ref)):
            result = lax.dot_general(
                rows_ref[...], rhs, (((1,), (1,)), ((), ())), preferred_element_type=F32
            )
            for m in range(count // 2):
                tile = result[:, m * 2 * width : (m + 1) * 2 * width]
                first = n * count + 2 * m
                out_ref[first + core] = tile.astype(BF)
                out_ref[first + 1 - core] = pltpu.roll(tile, width, 1).astype(BF)


def project(mine, partner, pieces):
    rows = mine.shape[0]
    count, _, width, _ = pieces[0].shape
    tiles = len(pieces) * count
    vmem = pl.BlockSpec(memory_space=pltpu.VMEM)
    out = jax.ShapeDtypeStruct((tiles, rows, 2 * width), BF)
    return pl.pallas_call(
        project_kernel,
        in_specs=[vmem] * (2 + len(pieces)),
        out_specs=[vmem, vmem],
        out_shape=[out, out],
        compiler_params=pltpu.CompilerParams(vmem_limit_bytes=6 << 20),
        cost_estimate=pl.CostEstimate(
            flops=4 * rows * width * tiles * mine.shape[1], bytes_accessed=4 << 20, transcendentals=0
        ),
        name="project",
    )(mine, partner, *pieces)


ORDER = (0, 1, 3, 2)


def merge_kernel(kept1, kept2, got1, got2, out_ref):
    index = lax.axis_index("dp")
    core, x, y = index & 1, (index >> 1) & 3, index >> 3
    first, second = lax.select(core == 0, x, y), lax.select(core == 0, y, x)
    step = out_ref.shape[0]
    width = kept1.shape[2]
    rows = pl.ds(pl.multiple_of(pl.program_id(0) * step, step), step)
    lane = lax.broadcasted_iota(jnp.int32, (step, width), 1)
    ours = (lane // (width // 2)) == core

    def tile(refs, r, j):
        place = ORDER.index(r)
        return refs[0][place * 4 + j, rows, :] if place < 3 else refs[1][j, rows, :]

    for r in range(4):
        a = lax.rem(first + r, 4)
        for t in range(4):
            b = lax.rem(second + t, 4)
            at = lax.select(core == 0, b * 4 + a, a * 4 + b)
            kept = tile((kept1, kept2), r, b).astype(F32)
            got = tile((got1, got2), t, a).astype(F32)
            where = pl.ds(pl.multiple_of(at * width, width), width)
            out_ref[:, where] = jnp.where(ours, kept, got).astype(BF)


def merge(kept1, kept2, got1, got2):
    rows, width = kept1.shape[1:]
    vmem = pl.BlockSpec(memory_space=pltpu.VMEM)
    return pl.pallas_call(
        merge_kernel,
        grid=(rows // BLOCK,),
        in_specs=[vmem] * 4,
        out_specs=pl.BlockSpec((BLOCK, 16 * width), lambda i: (i, 0)),
        out_shape=jax.ShapeDtypeStruct((rows, 16 * width), BF),
        compiler_params=pltpu.CompilerParams(vmem_limit_bytes=4 << 20),
        name="merge",
    )(kept1, kept2, got1, got2)


def at(y, x, core):
    return (y % 4 * 4 + x % 4) * 2 + core


GROUPS = [[at(y, x, 0) for y in range(4)] for x in range(4)] + [
    [at(y, x, 1) for x in range(4)] for y in range(4)
]


def ring(shift):
    pairs = []
    for y in range(4):
        for x in range(4):
            pairs.append((at(y, x, 0), at(y, x + shift, 0)))
            pairs.append((at(y, x, 1), at(y + shift, x, 1)))
    return pairs


SWAP = [(d, d ^ 1) for d in range(32)]


def sent_to_all(value, axis, length, groups=None):
    return lax.all_to_all(
        jnp.broadcast_to(value[None], (length, *value.shape)),
        axis,
        0,
        0,
        tiled=True,
        axis_index_groups=groups,
    )


def moved(value, pairs):
    return lax.ppermute(value, "dp", pairs)


def per_device(up_pre, mix_pre, ln_gain, mix_weight, mix_bias, out_weight):
    slab = sent_to_all(out_weight.T, "sp", 16)
    normed = norm(mix_pre[0], ln_gain[None])
    gated = gate(normed, up_pre[0], mix_weight, mix_bias)
    slab, gated = lax.optimization_barrier((slab, gated))
    own = sent_to_all(slab, "dp", 4, GROUPS)
    before = moved(own, ring(1))
    after = moved(own, ring(-1))
    across = moved(own, ring(2))
    partner = moved(gated, SWAP)
    kept1, sent1 = project(gated, partner, [own, after, before])
    across, kept1 = lax.optimization_barrier((across, kept1))
    got1 = moved(sent1, SWAP)
    kept2, sent2 = project(gated, partner, [across])
    got2 = moved(sent2, SWAP)
    return merge(kept1, kept2, got1, got2)[None]


def solution(mesh):
    return jax.shard_map(
        per_device,
        mesh=mesh,
        in_specs=(P("dp", "sp", None), P("dp", "sp", None), P(), P(), P(), P("sp", "dp")),
        out_specs=P("dp", "sp", None),
        check_vma=False,
    )
```

time: 101 us -> 100 us (0.990)
  waiting for transfers between devices: 29.4 us -> 33.7 us
  local copies, waits for them, and re-layouts: 8.67 us -> 4.81 us
  starting transfers between devices: 53 us -> 49.4 us
  Pallas kernels: 9.54 us -> 11.8 us
    ppermute x9 -> x6, waiting for transfers between devices: 16.4 us -> 24.7 us  [moved(): return lax.ppermute(value, 'dp', pairs)]
    all_to_all x2, waiting for transfers between devices: 13 us -> 8.96 us  [sent_to_all(): lax.all_to_all(jnp.broadcast_to(value[None], (length, *value.shape)), axi...]
    unnamed x19 -> x10, local copies, waits for them, and re-layouts: 5.89 us -> 2.11 us
    ppermute x9 -> x6, starting transfers between devices: 33.2 us -> 29.5 us  [moved(): return lax.ppermute(value, 'dp', pairs)]
    pallas_call x1 -> x3, Pallas kernels: 4.99 us -> 7.03 us  [the longest x2 5.02 us: project(): pl.pallas_call(project_kernel, in_specs=[vmem] * (2 + len(pieces)), out_s...]
  transfers between devices with their start and end apart: 11 -> 8, of which waited for: 5 -> 5; matrix products, arithmetic and copies ran while one was open for 0% -> 0% of each run, Pallas kernels for 5% -> 10%
where the time goes in v3:
time: 100 us; the launch traced here: 99.8 us
  starting transfers between devices  49.4 us (49%)
  waiting for transfers between devices  33.7 us (34%)
  Pallas kernels  11.8 us (12%)
  local copies, waits for them, and re-layouts  4.81 us (5%)
    ppermute x6, starting transfers between devices, moved(): return lax.ppermute(value, 'dp', pairs)  29.5 us
    ppermute x6, waiting for transfers between devices, moved(): return lax.ppermute(value, 'dp', pairs)  24.7 us
    all_to_all x2, starting transfers between devices, sent_to_all(): lax.all_to_all(jnp.broadcast_to(value[None], (length, *value.shape)), axi...  20 us
    all_to_all x2, waiting for transfers between devices, sent_to_all(): lax.all_to_all(jnp.broadcast_to(value[None], (length, *value.shape)), axi...  8.96 us
    pallas_call x2, Pallas kernels, project(): pl.pallas_call(project_kernel, in_specs=[vmem] * (2 + len(pieces)), out_s...  5.02 us
    pallas_call x1, Pallas kernels, norm(): pl.pallas_call(norm_kernel, grid=(rows // BLOCK,), in_specs=[pl.BlockSpec...  3.06 us
    broadcast_in_dim x2, local copies, waits for them, and re-layouts, sent_to_all(): jnp.broadcast_to(value[None], (length, *value.shape))  2.7 us
    unnamed x10, local copies, waits for them, and re-layouts  2.11 us
  transfers between devices with their start and end apart: 8, of which 5 were waited for; matrix products, arithmetic and copies ran while one was open for 0% of the time, Pallas kernels for 10%

profile of v3, /device:TPU:1, one launch (start us, length us, event | category | flops | bytes accessed | tf_op | source)
XLA Modules:
  0.0 99.8 jit_solution(9261643036763561507)
XLA Ops:
  0.0 1.5 %broadcast_in_dim.8 = bf16[16,64,128]{2,1,0:T(8,128)(2,1)} broadcast(bf16[64,128]{1,0:T(8,128)(2,1)} %bitcast.8), dimensions={1,2} | broadcast | bytes 278528 | tf_op jit(solution)/shard_map/broadcast_in_dim | solution.py:203
  1.5 15.7 %all-to-all-start = ((bf16[16,64,128]{2,1,0:T(8,128)(2,1)}), bf16[16,64,128]{2,1,0:T(8,128)(2,1)S(1)}, u32[]{:S(2)}, u32[]{:S(2)}) async-start(bf16[16,64,128]{2,1,0:T(8,128)(2,1)} %broadcast_in_dim.8), calls=%async_computation | async-start | bytes 524288 | tf_op jit(solution)/shard_map/all_to_all | solution.py:202
  17.2 0.0 copy-start
  17.2 1.4 %copy-done = bf16[1,384,2048]{2,1,0:T(8,128)(2,1)S(1)} copy-done((bf16[1,384,2048]{2,1,0:T(8,128)(2,1)S(1)}, bf16[1,384,2048]{2,1,0:T(8,128)(2,1)}, u32[]{:S(2)}) %copy-start) | copy-done | bytes 1572888
  18.6 0.7 copy-done.3
  19.3 3.1 %norm.1.normed_ref = bf16[384,2048]{1,0:T(8,128)(2,1)S(1)} custom-call(bf16[384,2048]{1,0:T(8,128)(2,1)S(1)} %bitcast.5, f32[1,2048]{1,0:T(1,128)S(1)} %bitcast.7), custom_call_target="tpu_custom_call" | custom-call | flops 4000000000 | bytes 3145728 | tf_op jit(solution)/shard_map/norm/pallas_call | solution.py:40
  22.4 1.7 %gate.1.mine_ref = bf16[384,2048]{1,0:T(8,128)(2,1)S(1)} custom-call(bf16[384,2048]{1,0:T(8,128)(2,1)S(1)} %norm.1.normed_ref, bf16[384,2048]{1,0:T(8,128)(2,1)S(1)} %bitcast.6, bf16[16,128,128]{2,1,0:T(8,128)(2,1)S(1)} %copy-done.2, f32[16,128]{1,0:T(8,128)S(1)} %copy-done.4), custom_call_target="tpu_custom_call" | custom-call | flops 4000000000 | bytes 4718592 | tf_op jit(solution)/shard_map/gate/pallas_call | solution.py:77
  24.1 6.8 %all-to-all-done = bf16[16,64,128]{2,1,0:T(8,128)(2,1)S(1)} async-done(((bf16[16,64,128]{2,1,0:T(8,128)(2,1)}), bf16[16,64,128]{2,1,0:T(8,128)(2,1)S(1)}, u32[]{:S(2)}, u32[]{:S(2)}) %all-to-all-start) | async-done | bytes 262176 | tf_op jit(solution)/shard_map/all_to_all | solution.py:202
  31.0 1.2 %broadcast_in_dim.20 = bf16[4,16,64,128]{3,2,1,0:T(8,128)(2,1)} broadcast(bf16[16,64,128]{2,1,0:T(8,128)(2,1)S(1)} %all-to-all-done), dimensions={1,2,3} | broadcast | bytes 1310720 | tf_op jit(solution)/shard_map/broadcast_in_dim | solution.py:203
  32.2 4.2 %all-to-all-start.1 = ((bf16[4,16,64,128]{3,2,1,0:T(8,128)(2,1)}), bf16[4,16,64,128]{3,2,1,0:T(8,128)(2,1)}, u32[]{:S(2)}, u32[]{:S(2)}) async-start(bf16[4,16,64,128]{3,2,1,0:T(8,128)(2,1)} %broadcast_in_dim.20), calls=%async_computation.1 | async-start | bytes 2097152 | tf_op jit(solution)/shard_map/all_to_all | solution.py:202
  36.5 7.7 %collective-permute-start.1 = (bf16[384,2048]{1,0:T(8,128)(2,1)S(1)}, bf16[384,2048]{1,0:T(8,128)(2,1)S(1)}, u32[]{:S(2)}, u32[]{:S(2)}) collective-permute-start(bf16[384,2048]{1,0:T(8,128)(2,1)S(1)} %gate.1.mine_ref), channel_id=1, source_target_pairs={{0,1},{1,0},{2,3},{3,2},{4,5},{5,4},{6,7},{7,6},{8,9},{9,8},{10,11... | collective-permute-start | bytes 4718600 | tf_op jit(solution)/shard_map/ppermute | solution.py:213
  44.1 2.1 %all-to-all-done.1.refs_0_ = bf16[4,16,64,128]{3,2,1,0:T(8,128)(2,1)} async-done(((bf16[4,16,64,128]{3,2,1,0:T(8,128)(2,1)}), bf16[4,16,64,128]{3,2,1,0:T(8,128)(2,1)}, u32[]{:S(2)}, u32[]{:S(2)}) %all-to-all-start.1) | async-done | bytes 1048608 | tf_op jit(solution)/shard_map/all_to_all | solution.py:202
  46.3 4.6 %collective-permute-start.2 = (bf16[4,16,64,128]{3,2,1,0:T(8,128)(2,1)}, bf16[4,16,64,128]{3,2,1,0:T(8,128)(2,1)S(1)}, u32[]{:S(2)}, u32[]{:S(2)}) collective-permute-start(bf16[4,16,64,128]{3,2,1,0:T(8,128)(2,1)} %all-to-all-done.1.refs_0_), channel_id=1, source_target_pairs={{0,6},{1,25},{2,0},{3,27},{4,2},{5,29},{6,4},{7,31},{8,14},{9,1},{... | collective-permute-start | bytes 3145736 | tf_op jit(solution)/shard_map/ppermute | solution.py:213
  50.9 1.9 %collective-permute-start.3 = (bf16[4,16,64,128]{3,2,1,0:T(8,128)(2,1)}, bf16[4,16,64,128]{3,2,1,0:T(8,128)(2,1)S(1)}, u32[]{:S(2)}, u32[]{:S(2)}) collective-permute-start(bf16[4,16,64,128]{3,2,1,0:T(8,128)(2,1)} %all-to-all-done.1.refs_0_), channel_id=1, source_target_pairs={{0,2},{1,9},{2,4},{3,11},{4,6},{5,13},{6,0},{7,15},{8,10},{9,17},{... | collective-permute-start | bytes 3145736 | tf_op jit(solution)/shard_map/ppermute | solution.py:213
  52.8 3.5 %collective-permute-start = (bf16[4,16,64,128]{3,2,1,0:T(8,128)(2,1)}, bf16[4,16,64,128]{3,2,1,0:T(8,128)(2,1)S(1)}, u32[]{:S(2)}, u32[]{:S(2)}) collective-permute-start(bf16[4,16,64,128]{3,2,1,0:T(8,128)(2,1)} %all-to-all-done.1.refs_0_), channel_id=1, source_target_pairs={{0,4},{1,17},{2,6},{3,19},{4,0},{5,21},{6,2},{7,23},{8,12},{9,25},... | collective-permute-start | bytes 3145736 | tf_op jit(solution)/shard_map/ppermute | solution.py:213
  56.4 0.0 collective-permute-done.1.partner_ref
  56.4 17.8 %collective-permute-done.2.refs_1_ = bf16[4,16,64,128]{3,2,1,0:T(8,128)(2,1)S(1)} collective-permute-done((bf16[4,16,64,128]{3,2,1,0:T(8,128)(2,1)}, bf16[4,16,64,128]{3,2,1,0:T(8,128)(2,1)S(1)}, u32[]{:S(2)}, u32[]{:S(2)}) %collective-permute-start.2) | collective-permute-done | bytes 1048608 | tf_op jit(solution)/shard_map/ppermute | solution.py:213
  74.2 5.2 %collective-permute-done.3.refs_2_ = bf16[4,16,64,128]{3,2,1,0:T(8,128)(2,1)S(1)} collective-permute-done((bf16[4,16,64,128]{3,2,1,0:T(8,128)(2,1)}, bf16[4,16,64,128]{3,2,1,0:T(8,128)(2,1)S(1)}, u32[]{:S(2)}, u32[]{:S(2)}) %collective-permute-start.3) | collective-permute-done | bytes 1048608 | tf_op jit(solution)/shard_map/ppermute | solution.py:213
  79.4 3.9 %project.2 = (bf16[12,384,128]{2,1,0:T(8,128)(2,1)S(1)}, bf16[12,384,128]{2,1,0:T(8,128)(2,1)S(1)}) custom-call(bf16[384,2048]{1,0:T(8,128)(2,1)S(1)} %gate.1.mine_ref, bf16[384,2048]{1,0:T(8,128)(2,1)S(1)} %collective-permute-done.1.partner_ref, bf16[4,16,64,128]{3,2,1,0:T(8,128)(2,1)} %all-to-all-done.1.refs_0_, ...), custom_call_target="tpu_custom_call" | custom-call | flops 2415919104 | bytes 4194304 | tf_op jit(solution)/shard_map/project/pallas_call | solution.py:125
  83.3 9.8 %collective-permute-start.4 = (bf16[12,384,128]{2,1,0:T(8,128)(2,1)S(1)}, bf16[12,384,128]{2,1,0:T(8,128)(2,1)S(1)}, u32[]{:S(2)}, u32[]{:S(2)}) collective-permute-start(bf16[12,384,128]{2,1,0:T(8,128)(2,1)S(1)} %get-tuple-element.19), channel_id=1, source_target_pairs={{0,1},{1,0},{2,3},{3,2},{4,5},{5,4},{6,7},{7,6},{8,9},{9,8},{10,11... | collective-permute-start | bytes 3538952 | tf_op jit(solution)/shard_map/ppermute | solution.py:213
  93.1 1.1 %project.3 = (bf16[4,384,128]{2,1,0:T(8,128)(2,1)S(1)}, bf16[4,384,128]{2,1,0:T(8,128)(2,1)S(1)}) custom-call(bf16[384,2048]{1,0:T(8,128)(2,1)S(1)} %gate.1.mine_ref, bf16[384,2048]{1,0:T(8,128)(2,1)S(1)} %collective-permute-done.1.partner_ref, bf16[4,16,64,128]{3,2,1,0:T(8,128)(2,1)S(1)} %collective-permute-done.refs_0_), custom_call_target="tpu_custom_call" | custom-call | flops 805306368 | bytes 4194304 | tf_op jit(solution)/shard_map/project/pallas_call | solution.py:125
  94.2 1.9 %collective-permute-start.5 = (bf16[4,384,128]{2,1,0:T(8,128)(2,1)S(1)}, bf16[4,384,128]{2,1,0:T(8,128)(2,1)S(1)}, u32[]{:S(2)}, u32[]{:S(2)}) collective-permute-start(bf16[4,384,128]{2,1,0:T(8,128)(2,1)S(1)} %get-tuple-element.20), channel_id=1, source_target_pairs={{0,1},{1,0},{2,3},{3,2},{4,5},{5,4},{6,7},{7,6},{8,9},{9,8},{10,11... | collective-permute-start | bytes 1179656 | tf_op jit(solution)/shard_map/ppermute | solution.py:213
  96.1 1.7 %collective-permute-done.5.got2 = bf16[4,384,128]{2,1,0:T(8,128)(2,1)S(1)} collective-permute-done((bf16[4,384,128]{2,1,0:T(8,128)(2,1)S(1)}, bf16[4,384,128]{2,1,0:T(8,128)(2,1)S(1)}, u32[]{:S(2)}, u32[]{:S(2)}) %collective-permute-start.5) | collective-permute-done | bytes 393248 | tf_op jit(solution)/shard_map/ppermute | solution.py:213
  97.8 2.0 %merge.1 = bf16[384,2048]{1,0:T(8,128)(2,1)} custom-call(bf16[12,384,128]{2,1,0:T(8,128)(2,1)S(1)} %get-tuple-element.16.kept1, bf16[4,384,128]{2,1,0:T(8,128)(2,1)S(1)} %get-tuple-element.18.kept2, bf16[12,384,128]{2,1,0:T(8,128)(2,1)S(1)} %collective-permute-done.4.got1, bf16[4,384,128]{2,1,0:T(8,128)(2,1)S(1)} %collective-permute-done.5.got2), custom_call_target="tpu_custom_call" | custom-call | tf_op jit(solution)/shard_map/merge/pallas_call | solution.py:169
  (9 shorter events, 0.0 us)
Async XLA Ops:
  1.5 29.5 %all-to-all-start = ((bf16[16,64,128]{2,1,0:T(8,128)(2,1)}), bf16[16,64,128]{2,1,0:T(8,128)(2,1)S(1)}, u32[]{:S(2)}, u32[]{:S(2)}) async-start(bf16[16,64,128]{2,1,0:T(8,128)(2,1)} %broadcast_in_dim.8), calls=%async_computation | async-start | bytes 524288 | tf_op jit(solution)/shard_map/all_to_all | solution.py:202
  17.2 1.4 %copy-start = (bf16[1,384,2048]{2,1,0:T(8,128)(2,1)S(1)}, bf16[1,384,2048]{2,1,0:T(8,128)(2,1)}, u32[]{:S(2)}) copy-start(bf16[1,384,2048]{2,1,0:T(8,128)(2,1)} %param.7) | copy-start | bytes 4718596
  18.6 0.7 copy-start.3
  19.3 3.1 %copy-start.1 = (bf16[1,384,2048]{2,1,0:T(8,128)(2,1)S(1)}, bf16[1,384,2048]{2,1,0:T(8,128)(2,1)}, u32[]{:S(2)}) copy-start(bf16[1,384,2048]{2,1,0:T(8,128)(2,1)} %param.6) | copy-start | bytes 4718596
  19.3 3.1 %copy-start.2 = (bf16[16,128,128]{2,1,0:T(8,128)(2,1)S(1)}, bf16[16,128,128]{2,1,0:T(8,128)(2,1)}, u32[]{:S(2)}) copy-start(bf16[16,128,128]{2,1,0:T(8,128)(2,1)} %weight_ref.1) | copy-start | bytes 1572868
  19.3 3.1 %copy-start.4 = (f32[16,128]{1,0:T(8,128)S(1)}, f32[16,128]{1,0:T(8,128)}, u32[]{:S(2)}) copy-start(f32[16,128]{1,0:T(8,128)} %bias_ref.1) | copy-start | bytes 24580
  32.2 14.0 %all-to-all-start.1 = ((bf16[4,16,64,128]{3,2,1,0:T(8,128)(2,1)}), bf16[4,16,64,128]{3,2,1,0:T(8,128)(2,1)}, u32[]{:S(2)}, u32[]{:S(2)}) async-start(bf16[4,16,64,128]{3,2,1,0:T(8,128)(2,1)} %broadcast_in_dim.20), calls=%async_computation.1 | async-start | bytes 2097152 | tf_op jit(solution)/shard_map/all_to_all | solution.py:202
  36.5 19.9 %collective-permute-start.1 = (bf16[384,2048]{1,0:T(8,128)(2,1)S(1)}, bf16[384,2048]{1,0:T(8,128)(2,1)S(1)}, u32[]{:S(2)}, u32[]{:S(2)}) collective-permute-start(bf16[384,2048]{1,0:T(8,128)(2,1)S(1)} %gate.1.mine_ref), channel_id=1, source_target_pairs={{0,1},{1,0},{2,3},{3,2},{4,5},{5,4},{6,7},{7,6},{8,9},{9,8},{10,11... | collective-permute-start | bytes 4718600 | tf_op jit(solution)/shard_map/ppermute | solution.py:213
  46.3 27.9 %collective-permute-start.2 = (bf16[4,16,64,128]{3,2,1,0:T(8,128)(2,1)}, bf16[4,16,64,128]{3,2,1,0:T(8,128)(2,1)S(1)}, u32[]{:S(2)}, u32[]{:S(2)}) collective-permute-start(bf16[4,16,64,128]{3,2,1,0:T(8,128)(2,1)} %all-to-all-done.1.refs_0_), channel_id=1, source_target_pairs={{0,6},{1,25},{2,0},{3,27},{4,2},{5,29},{6,4},{7,31},{8,14},{9,1},{... | collective-permute-start | bytes 3145736 | tf_op jit(solution)/shard_map/ppermute | solution.py:213
  50.9 28.5 %collective-permute-start.3 = (bf16[4,16,64,128]{3,2,1,0:T(8,128)(2,1)}, bf16[4,16,64,128]{3,2,1,0:T(8,128)(2,1)S(1)}, u32[]{:S(2)}, u32[]{:S(2)}) collective-permute-start(bf16[4,16,64,128]{3,2,1,0:T(8,128)(2,1)} %all-to-all-done.1.refs_0_), channel_id=1, source_target_pairs={{0,2},{1,9},{2,4},{3,11},{4,6},{5,13},{6,0},{7,15},{8,10},{9,17},{... | collective-permute-start | bytes 3145736 | tf_op jit(solution)/shard_map/ppermute | solution.py:213
  52.8 40.3 %collective-permute-start = (bf16[4,16,64,128]{3,2,1,0:T(8,128)(2,1)}, bf16[4,16,64,128]{3,2,1,0:T(8,128)(2,1)S(1)}, u32[]{:S(2)}, u32[]{:S(2)}) collective-permute-start(bf16[4,16,64,128]{3,2,1,0:T(8,128)(2,1)} %all-to-all-done.1.refs_0_), channel_id=1, source_target_pairs={{0,4},{1,17},{2,6},{3,19},{4,0},{5,21},{6,2},{7,23},{8,12},{9,25},... | collective-permute-start | bytes 3145736 | tf_op jit(solution)/shard_map/ppermute | solution.py:213
  83.3 14.5 %collective-permute-start.4 = (bf16[12,384,128]{2,1,0:T(8,128)(2,1)S(1)}, bf16[12,384,128]{2,1,0:T(8,128)(2,1)S(1)}, u32[]{:S(2)}, u32[]{:S(2)}) collective-permute-start(bf16[12,384,128]{2,1,0:T(8,128)(2,1)S(1)} %get-tuple-element.19), channel_id=1, source_target_pairs={{0,1},{1,0},{2,3},{3,2},{4,5},{5,4},{6,7},{7,6},{8,9},{9,8},{10,11... | collective-permute-start | bytes 3538952 | tf_op jit(solution)/shard_map/ppermute | solution.py:213
  94.2 3.6 %collective-permute-start.5 = (bf16[4,384,128]{2,1,0:T(8,128)(2,1)S(1)}, bf16[4,384,128]{2,1,0:T(8,128)(2,1)S(1)}, u32[]{:S(2)}, u32[]{:S(2)}) collective-permute-start(bf16[4,384,128]{2,1,0:T(8,128)(2,1)S(1)} %get-tuple-element.20), channel_id=1, source_target_pairs={{0,1},{1,0},{2,3},{3,2},{4,5},{5,4},{6,7},{7,6},{8,9},{9,8},{10,11... | collective-permute-start | bytes 1179656 | tf_op jit(solution)/shard_map/ppermute | solution.py:213

commit v4 on v3

--- a/solution.py
+++ b/solution.py
@@ -1,3 +1,5 @@
+import functools
+
 import jax
 import jax.numpy as jnp
 from jax import lax
@@ -93,14 +95,15 @@
     )(normed, up, weight, bias)
 
 
-def project_kernel(mine_ref, partner_ref, *refs):
-    pieces, kept_ref, sent_ref = refs[:-2], refs[-2], refs[-1]
+def project_kernel(split, mine_ref, partner_ref, *refs):
+    parts, kept_ref, sent_ref = refs[:-2], refs[-2], refs[-1]
     core = lax.axis_index("dp") & 1
-    for n, piece in enumerate(pieces):
-        count, blocks, width, _ = piece.shape
+    for n in range(len(parts) // split):
+        piece = parts[n * split : (n + 1) * split]
+        count, blocks, width, _ = piece[0].shape
         rhs = jnp.concatenate(
             [
-                jnp.concatenate([piece[j, k] for k in range(blocks)], axis=1)
+                jnp.concatenate([p[j, k] for p in piece for k in range(blocks)], axis=1)
                 for j in range(count)
             ],
             axis=0,
@@ -116,15 +119,15 @@
                 out_ref[first + 1 - core] = pltpu.roll(tile, width, 1).astype(BF)
 
 
-def project(mine, partner, pieces):
+def project(mine, partner, parts, split):
     rows = mine.shape[0]
-    count, _, width, _ = pieces[0].shape
-    tiles = len(pieces) * count
+    count, _, width, _ = parts[0].shape
+    tiles = len(parts) // split * count
     vmem = pl.BlockSpec(memory_space=pltpu.VMEM)
     out = jax.ShapeDtypeStruct((tiles, rows, 2 * width), BF)
     return pl.pallas_call(
-        project_kernel,
-        in_specs=[vmem] * (2 + len(pieces)),
+        functools.partial(project_kernel, split),
+        in_specs=[vmem] * (2 + len(parts)),
         out_specs=[vmem, vmem],
         out_shape=[out, out],
         compiler_params=pltpu.CompilerParams(vmem_limit_bytes=6 << 20),
@@ -132,7 +135,7 @@
             flops=4 * rows * width * tiles * mine.shape[1], bytes_accessed=4 << 20, transcendentals=0
         ),
         name="project",
-    )(mine, partner, *pieces)
+    )(mine, partner, *parts)
 
 
 ORDER = (0, 1, 3, 2)
@@ -217,16 +220,17 @@
     slab = sent_to_all(out_weight.T, "sp", 16)
     normed = norm(mix_pre[0], ln_gain[None])
     gated = gate(normed, up_pre[0], mix_weight, mix_bias)
-    slab, gated = lax.optimization_barrier((slab, gated))
+    partner = moved(gated, SWAP)
+    slab, partner = lax.optimization_barrier((slab, partner))
     own = sent_to_all(slab, "dp", 4, GROUPS)
     before = moved(own, ring(1))
     after = moved(own, ring(-1))
-    across = moved(own, ring(2))
-    partner = moved(gated, SWAP)
-    kept1, sent1 = project(gated, partner, [own, after, before])
-    across, kept1 = lax.optimization_barrier((across, kept1))
+    low2 = moved(before[:, :8], ring(1))
+    high2 = moved(after[:, 8:], ring(-1))
+    kept1, sent1 = project(gated, partner, [own, after, before], 1)
     got1 = moved(sent1, SWAP)
-    kept2, sent2 = project(gated, partner, [across])
+    low2, high2, kept1 = lax.optimization_barrier((low2, high2, kept1))
+    kept2, sent2 = project(gated, partner, [low2, high2], 2)
     got2 = moved(sent2, SWAP)
     return merge(kept1, kept2, got1, got2)[None]
 

time: 100 us -> 107 us (1.070)
  blocking collectives: 0 us -> 37.3 us
  waiting for transfers between devices: 33.7 us -> 19.6 us
  starting transfers between devices: 49.4 us -> 36 us
  local copies, waits for them, and re-layouts: 4.81 us -> 2.48 us
  Pallas kernels: 11.8 us -> 10.6 us
    all_to_all x0 -> x2, blocking collectives: none -> 37.3 us  [sent_to_all(): lax.all_to_all(jnp.broadcast_to(value[None], (length, *value.shape)), axi...]
    all_to_all x2 -> x0, starting transfers between devices: 20 us -> none  [sent_to_all(): lax.all_to_all(jnp.broadcast_to(value[None], (length, *value.shape)), axi...]
    all_to_all x2 -> x0, waiting for transfers between devices: 8.96 us -> none  [sent_to_all(): lax.all_to_all(jnp.broadcast_to(value[None], (length, *value.shape)), axi...]
    ppermute x6 -> x7, starting transfers between devices: 29.5 us -> 36 us  [moved(): return lax.ppermute(value, 'dp', pairs)]
    ppermute x6 -> x7, waiting for transfers between devices: 24.7 us -> 19.6 us  [moved(): return lax.ppermute(value, 'dp', pairs)]
    broadcast_in_dim x2, local copies, waits for them, and re-layouts: 2.7 us -> 0.29 us  [sent_to_all(): jnp.broadcast_to(value[None], (length, *value.shape))]
    pallas_call x2, Pallas kernels: 5.02 us -> 3.79 us  [project(): pl.pallas_call(functools.partial(project_kernel, split), in_specs=[vmem]...]
  transfers between devices with their start and end apart: 8 -> 7, of which waited for: 5 -> 5; matrix products, arithmetic and copies ran while one was open for 0% -> 0% of each run, Pallas kernels for 10% -> 1%
where the time goes in v4:
time: 107 us; the launch traced here: 106 us
  blocking collectives  37.3 us (35%)
  starting transfers between devices  36 us (34%)
  waiting for transfers between devices  19.6 us (18%)
  Pallas kernels  10.6 us (10%)
  local copies, waits for them, and re-layouts  2.48 us (2%)
    all_to_all x2, blocking collectives, sent_to_all(): lax.all_to_all(jnp.broadcast_to(value[None], (length, *value.shape)), axi...  37.3 us
    ppermute x7, starting transfers between devices, moved(): return lax.ppermute(value, 'dp', pairs)  36 us
    ppermute x7, waiting for transfers between devices, moved(): return lax.ppermute(value, 'dp', pairs)  19.6 us
    pallas_call x2, Pallas kernels, project(): pl.pallas_call(functools.partial(project_kernel, split), in_specs=[vmem]...  3.79 us
    pallas_call x1, Pallas kernels, norm(): pl.pallas_call(norm_kernel, grid=(rows // BLOCK,), in_specs=[pl.BlockSpec...  3.06 us
  transfers between devices with their start and end apart: 7, of which 5 were waited for; matrix products, arithmetic and copies ran while one was open for 0% of the time, Pallas kernels for 1%

profile of v4, /device:TPU:1, one launch (start us, length us, event | category | flops | bytes accessed | tf_op | source)
XLA Modules:
  0.0 106.2 jit_solution(9066008450933088263)
XLA Ops:
  0.0 1.4 %copy-done = bf16[1,384,2048]{2,1,0:T(8,128)(2,1)S(1)} copy-done((bf16[1,384,2048]{2,1,0:T(8,128)(2,1)S(1)}, bf16[1,384,2048]{2,1,0:T(8,128)(2,1)}, u32[]{:S(2)}) %copy-start) | copy-done | bytes 1572888
  1.4 0.7 copy-done.3
  2.1 3.1 %norm.1.normed_ref = bf16[384,2048]{1,0:T(8,128)(2,1)S(1)} custom-call(bf16[384,2048]{1,0:T(8,128)(2,1)S(1)} %bitcast.5, f32[1,2048]{1,0:T(1,128)S(1)} %bitcast.7), custom_call_target="tpu_custom_call" | custom-call | flops 4000000000 | bytes 3145728 | tf_op jit(solution)/shard_map/norm/pallas_call | solution.py:42
  5.2 0.0 copy-start.5
  5.2 1.7 %gate.1.mine_ref = bf16[384,2048]{1,0:T(8,128)(2,1)S(1)} custom-call(bf16[384,2048]{1,0:T(8,128)(2,1)S(1)} %norm.1.normed_ref, bf16[384,2048]{1,0:T(8,128)(2,1)S(1)} %bitcast.6, bf16[16,128,128]{2,1,0:T(8,128)(2,1)S(1)} %copy-done.2, f32[16,128]{1,0:T(8,128)S(1)} %copy-done.4), custom_call_target="tpu_custom_call" | custom-call | flops 4000000000 | bytes 4718592 | tf_op jit(solution)/shard_map/gate/pallas_call | solution.py:79
  6.9 8.7 %collective-permute-start = (bf16[384,2048]{1,0:T(8,128)(2,1)S(1)}, bf16[384,2048]{1,0:T(8,128)(2,1)S(1)}, u32[]{:S(2)}, u32[]{:S(2)}) collective-permute-start(bf16[384,2048]{1,0:T(8,128)(2,1)S(1)} %gate.1.mine_ref), channel_id=1, source_target_pairs={{0,1},{1,0},{2,3},{3,2},{4,5},{5,4},{6,7},{7,6},{8,9},{9,8},{10,11... | collective-permute-start | bytes 4718600 | tf_op jit(solution)/shard_map/ppermute | solution.py:216
  15.8 23.7 %all_to_all.10 = bf16[16,64,128]{2,1,0:T(8,128)(2,1)S(1)} all-to-all(bf16[16,64,128]{2,1,0:T(8,128)(2,1)S(1)} %broadcast_in_dim.8), channel_id=1, replica_groups=mesh['sp'=16,'dp'=32] {'sp'}, dimensions={0} | all-to-all | bytes 524288 | tf_op jit(solution)/shard_map/all_to_all | solution.py:205
  39.5 0.0 collective-permute-done.partner_ref
  39.5 0.2 broadcast_in_dim.20
  39.7 13.6 %all_to_all.11.refs_0_ = bf16[4,16,64,128]{3,2,1,0:T(8,128)(2,1)S(1)} all-to-all(bf16[4,16,64,128]{3,2,1,0:T(8,128)(2,1)S(1)} %broadcast_in_dim.20), channel_id=1, replica_groups={{0,8,16,24},{2,10,18,26},{4,12,20,28},{6,14,22,30},{1,3,5,7},{9,11,13,1..., dimensions={0} | all-to-all | bytes 2097152 | tf_op jit(solution)/shard_map/all_to_all | solution.py:205
  53.3 3.2 %collective-permute-start.1 = (bf16[4,16,64,128]{3,2,1,0:T(8,128)(2,1)S(1)}, bf16[4,16,64,128]{3,2,1,0:T(8,128)(2,1)S(1)}, u32[]{:S(2)}, u32[]{:S(2)}) collective-permute-start(bf16[4,16,64,128]{3,2,1,0:T(8,128)(2,1)S(1)} %all_to_all.11.refs_0_), channel_id=1, source_target_pairs={{0,2},{1,9},{2,4},{3,11},{4,6},{5,13},{6,0},{7,15},{8,10},{9,17},{... | collective-permute-start | bytes 3145736 | tf_op jit(solution)/shard_map/ppermute | solution.py:216
  56.5 3.7 %collective-permute-start.3 = (bf16[4,16,64,128]{3,2,1,0:T(8,128)(2,1)S(1)}, bf16[4,16,64,128]{3,2,1,0:T(8,128)(2,1)S(1)}, u32[]{:S(2)}, u32[]{:S(2)}) collective-permute-start(bf16[4,16,64,128]{3,2,1,0:T(8,128)(2,1)S(1)} %all_to_all.11.refs_0_), channel_id=1, source_target_pairs={{0,6},{1,25},{2,0},{3,27},{4,2},{5,29},{6,4},{7,31},{8,14},{9,1},{... | collective-permute-start | bytes 3145736 | tf_op jit(solution)/shard_map/ppermute | solution.py:216
  60.1 10.5 %collective-permute-done.1.refs_2_ = bf16[4,16,64,128]{3,2,1,0:T(8,128)(2,1)S(1)} collective-permute-done((bf16[4,16,64,128]{3,2,1,0:T(8,128)(2,1)S(1)}, bf16[4,16,64,128]{3,2,1,0:T(8,128)(2,1)S(1)}, u32[]{:S(2)}, u32[]{:S(2)}) %collective-permute-start.1) | collective-permute-done | bytes 1048608 | tf_op jit(solution)/shard_map/ppermute | solution.py:216
  70.7 1.6 %collective-permute-done.3.refs_1_ = bf16[4,16,64,128]{3,2,1,0:T(8,128)(2,1)S(1)} collective-permute-done((bf16[4,16,64,128]{3,2,1,0:T(8,128)(2,1)S(1)}, bf16[4,16,64,128]{3,2,1,0:T(8,128)(2,1)S(1)}, u32[]{:S(2)}, u32[]{:S(2)}) %collective-permute-start.3) | collective-permute-done | bytes 1048608 | tf_op jit(solution)/shard_map/ppermute | solution.py:216
  72.3 2.7 %project.2 = (bf16[12,384,128]{2,1,0:T(8,128)(2,1)S(1)}, bf16[12,384,128]{2,1,0:T(8,128)(2,1)S(1)}) custom-call(bf16[384,2048]{1,0:T(8,128)(2,1)S(1)} %gate.1.mine_ref, bf16[384,2048]{1,0:T(8,128)(2,1)S(1)} %collective-permute-done.partner_ref, bf16[4,16,64,128]{3,2,1,0:T(8,128)(2,1)S(1)} %all_to_all.11.refs_0_, ...), custom_call_target="tpu_custom_call" | custom-call | flops 2415919104 | bytes 4194304 | tf_op jit(solution)/shard_map/project/pallas_call | solution.py:128
  75.0 9.7 %collective-permute-start.5 = (bf16[12,384,128]{2,1,0:T(8,128)(2,1)S(1)}, bf16[12,384,128]{2,1,0:T(8,128)(2,1)S(1)}, u32[]{:S(2)}, u32[]{:S(2)}) collective-permute-start(bf16[12,384,128]{2,1,0:T(8,128)(2,1)S(1)} %get-tuple-element.21), channel_id=1, source_target_pairs={{0,1},{1,0},{2,3},{3,2},{4,5},{5,4},{6,7},{7,6},{8,9},{9,8},{10,11... | collective-permute-start | bytes 3538952 | tf_op jit(solution)/shard_map/ppermute | solution.py:216
  84.7 1.9 %collective-permute-start.2 = (bf16[4,8,64,128]{3,2,1,0:T(8,128)(2,1)S(1)}, bf16[4,8,64,128]{3,2,1,0:T(8,128)(2,1)S(1)}, u32[]{:S(2)}, u32[]{:S(2)}) collective-permute-start(bf16[4,8,64,128]{3,2,1,0:T(8,128)(2,1)S(1)} %slice.8), channel_id=1, source_target_pairs={{0,2},{1,9},{2,4},{3,11},{4,6},{5,13},{6,0},{7,15},{8,10},{9,17},{... | collective-permute-start | bytes 1572872 | tf_op jit(solution)/shard_map/ppermute | solution.py:216
  86.7 4.6 %collective-permute-start.4 = (bf16[4,8,64,128]{3,2,1,0:T(8,128)(2,1)S(1)}, bf16[4,8,64,128]{3,2,1,0:T(8,128)(2,1)S(1)}, u32[]{:S(2)}, u32[]{:S(2)}) collective-permute-start(bf16[4,8,64,128]{3,2,1,0:T(8,128)(2,1)S(1)} %slice.9), channel_id=1, source_target_pairs={{0,6},{1,25},{2,0},{3,27},{4,2},{5,29},{6,4},{7,31},{8,14},{9,1},{... | collective-permute-start | bytes 1572872 | tf_op jit(solution)/shard_map/ppermute | solution.py:216
  91.3 4.9 %collective-permute-done.2.refs_0_ = bf16[4,8,64,128]{3,2,1,0:T(8,128)(2,1)S(1)} collective-permute-done((bf16[4,8,64,128]{3,2,1,0:T(8,128)(2,1)S(1)}, bf16[4,8,64,128]{3,2,1,0:T(8,128)(2,1)S(1)}, u32[]{:S(2)}, u32[]{:S(2)}) %collective-permute-start.2) | collective-permute-done | bytes 524320 | tf_op jit(solution)/shard_map/ppermute | solution.py:216
  96.2 1.2 %collective-permute-done.4.refs_1_ = bf16[4,8,64,128]{3,2,1,0:T(8,128)(2,1)S(1)} collective-permute-done((bf16[4,8,64,128]{3,2,1,0:T(8,128)(2,1)S(1)}, bf16[4,8,64,128]{3,2,1,0:T(8,128)(2,1)S(1)}, u32[]{:S(2)}, u32[]{:S(2)}) %collective-permute-start.4) | collective-permute-done | bytes 524320 | tf_op jit(solution)/shard_map/ppermute | solution.py:216
  97.4 1.1 %project.3 = (bf16[4,384,128]{2,1,0:T(8,128)(2,1)S(1)}, bf16[4,384,128]{2,1,0:T(8,128)(2,1)S(1)}) custom-call(bf16[384,2048]{1,0:T(8,128)(2,1)S(1)} %gate.1.mine_ref, bf16[384,2048]{1,0:T(8,128)(2,1)S(1)} %collective-permute-done.partner_ref, bf16[4,8,64,128]{3,2,1,0:T(8,128)(2,1)S(1)} %collective-permute-done.2.refs_0_, ...), custom_call_target="tpu_custom_call" | custom-call | flops 805306368 | bytes 4194304 | tf_op jit(solution)/shard_map/project/pallas_call | solution.py:128
  98.5 4.3 %collective-permute-start.6 = (bf16[4,384,128]{2,1,0:T(8,128)(2,1)S(1)}, bf16[4,384,128]{2,1,0:T(8,128)(2,1)S(1)}, u32[]{:S(2)}, u32[]{:S(2)}) collective-permute-start(bf16[4,384,128]{2,1,0:T(8,128)(2,1)S(1)} %get-tuple-element.22), channel_id=1, source_target_pairs={{0,1},{1,0},{2,3},{3,2},{4,5},{5,4},{6,7},{7,6},{8,9},{9,8},{10,11... | collective-permute-start | bytes 1179656 | tf_op jit(solution)/shard_map/ppermute | solution.py:216
  102.8 1.3 %collective-permute-done.6.got2 = bf16[4,384,128]{2,1,0:T(8,128)(2,1)S(1)} collective-permute-done((bf16[4,384,128]{2,1,0:T(8,128)(2,1)S(1)}, bf16[4,384,128]{2,1,0:T(8,128)(2,1)S(1)}, u32[]{:S(2)}, u32[]{:S(2)}) %collective-permute-start.6) | collective-permute-done | bytes 393248 | tf_op jit(solution)/shard_map/ppermute | solution.py:216
  104.1 2.0 %merge.1 = bf16[384,2048]{1,0:T(8,128)(2,1)} custom-call(bf16[12,384,128]{2,1,0:T(8,128)(2,1)S(1)} %get-tuple-element.17.kept1, bf16[4,384,128]{2,1,0:T(8,128)(2,1)S(1)} %get-tuple-element.20.kept2, bf16[12,384,128]{2,1,0:T(8,128)(2,1)S(1)} %collective-permute-done.5.got1, bf16[4,384,128]{2,1,0:T(8,128)(2,1)S(1)} %collective-permute-done.6.got2), custom_call_target="tpu_custom_call" | custom-call | tf_op jit(solution)/shard_map/merge/pallas_call | solution.py:172
  (13 shorter events, 0.1 us)
Async XLA Ops:
  0.0 1.4 %copy-start = (bf16[1,384,2048]{2,1,0:T(8,128)(2,1)S(1)}, bf16[1,384,2048]{2,1,0:T(8,128)(2,1)}, u32[]{:S(2)}) copy-start(bf16[1,384,2048]{2,1,0:T(8,128)(2,1)} %param.7) | copy-start | bytes 4718596
  1.4 0.7 copy-start.3
  2.1 3.1 %copy-start.1 = (bf16[1,384,2048]{2,1,0:T(8,128)(2,1)S(1)}, bf16[1,384,2048]{2,1,0:T(8,128)(2,1)}, u32[]{:S(2)}) copy-start(bf16[1,384,2048]{2,1,0:T(8,128)(2,1)} %param.6) | copy-start | bytes 4718596
  2.1 3.1 %copy-start.2 = (bf16[16,128,128]{2,1,0:T(8,128)(2,1)S(1)}, bf16[16,128,128]{2,1,0:T(8,128)(2,1)}, u32[]{:S(2)}) copy-start(bf16[16,128,128]{2,1,0:T(8,128)(2,1)} %weight_ref.1) | copy-start | bytes 1572868
  2.1 3.1 %copy-start.4 = (f32[16,128]{1,0:T(8,128)S(1)}, f32[16,128]{1,0:T(8,128)}, u32[]{:S(2)}) copy-start(f32[16,128]{1,0:T(8,128)} %bias_ref.1) | copy-start | bytes 24580
  5.2 10.5 %copy-start.5 = (bf16[128,64]{0,1:T(8,128)(2,1)S(1)}, bf16[128,64]{0,1:T(8,128)(2,1)}, u32[]{:S(2)}) copy-start(bf16[128,64]{0,1:T(8,128)(2,1)} %param.11) | copy-start | bytes 49156
  6.9 32.5 %collective-permute-start = (bf16[384,2048]{1,0:T(8,128)(2,1)S(1)}, bf16[384,2048]{1,0:T(8,128)(2,1)S(1)}, u32[]{:S(2)}, u32[]{:S(2)}) collective-permute-start(bf16[384,2048]{1,0:T(8,128)(2,1)S(1)} %gate.1.mine_ref), channel_id=1, source_target_pairs={{0,1},{1,0},{2,3},{3,2},{4,5},{5,4},{6,7},{7,6},{8,9},{9,8},{10,11... | collective-permute-start | bytes 4718600 | tf_op jit(solution)/shard_map/ppermute | solution.py:216
  53.3 17.4 %collective-permute-start.1 = (bf16[4,16,64,128]{3,2,1,0:T(8,128)(2,1)S(1)}, bf16[4,16,64,128]{3,2,1,0:T(8,128)(2,1)S(1)}, u32[]{:S(2)}, u32[]{:S(2)}) collective-permute-start(bf16[4,16,64,128]{3,2,1,0:T(8,128)(2,1)S(1)} %all_to_all.11.refs_0_), channel_id=1, source_target_pairs={{0,2},{1,9},{2,4},{3,11},{4,6},{5,13},{6,0},{7,15},{8,10},{9,17},{... | collective-permute-start | bytes 3145736 | tf_op jit(solution)/shard_map/ppermute | solution.py:216
  56.5 15.8 %collective-permute-start.3 = (bf16[4,16,64,128]{3,2,1,0:T(8,128)(2,1)S(1)}, bf16[4,16,64,128]{3,2,1,0:T(8,128)(2,1)S(1)}, u32[]{:S(2)}, u32[]{:S(2)}) collective-permute-start(bf16[4,16,64,128]{3,2,1,0:T(8,128)(2,1)S(1)} %all_to_all.11.refs_0_), channel_id=1, source_target_pairs={{0,6},{1,25},{2,0},{3,27},{4,2},{5,29},{6,4},{7,31},{8,14},{9,1},{... | collective-permute-start | bytes 3145736 | tf_op jit(solution)/shard_map/ppermute | solution.py:216
  75.0 29.1 %collective-permute-start.5 = (bf16[12,384,128]{2,1,0:T(8,128)(2,1)S(1)}, bf16[12,384,128]{2,1,0:T(8,128)(2,1)S(1)}, u32[]{:S(2)}, u32[]{:S(2)}) collective-permute-start(bf16[12,384,128]{2,1,0:T(8,128)(2,1)S(1)} %get-tuple-element.21), channel_id=1, source_target_pairs={{0,1},{1,0},{2,3},{3,2},{4,5},{5,4},{6,7},{7,6},{8,9},{9,8},{10,11... | collective-permute-start | bytes 3538952 | tf_op jit(solution)/shard_map/ppermute | solution.py:216
  84.7 11.4 %collective-permute-start.2 = (bf16[4,8,64,128]{3,2,1,0:T(8,128)(2,1)S(1)}, bf16[4,8,64,128]{3,2,1,0:T(8,128)(2,1)S(1)}, u32[]{:S(2)}, u32[]{:S(2)}) collective-permute-start(bf16[4,8,64,128]{3,2,1,0:T(8,128)(2,1)S(1)} %slice.8), channel_id=1, source_target_pairs={{0,2},{1,9},{2,4},{3,11},{4,6},{5,13},{6,0},{7,15},{8,10},{9,17},{... | collective-permute-start | bytes 1572872 | tf_op jit(solution)/shard_map/ppermute | solution.py:216
  86.7 10.7 %collective-permute-start.4 = (bf16[4,8,64,128]{3,2,1,0:T(8,128)(2,1)S(1)}, bf16[4,8,64,128]{3,2,1,0:T(8,128)(2,1)S(1)}, u32[]{:S(2)}, u32[]{:S(2)}) collective-permute-start(bf16[4,8,64,128]{3,2,1,0:T(8,128)(2,1)S(1)} %slice.9), channel_id=1, source_target_pairs={{0,6},{1,25},{2,0},{3,27},{4,2},{5,29},{6,4},{7,31},{8,14},{9,1},{... | collective-permute-start | bytes 1572872 | tf_op jit(solution)/shard_map/ppermute | solution.py:216
  98.5 5.6 %collective-permute-start.6 = (bf16[4,384,128]{2,1,0:T(8,128)(2,1)S(1)}, bf16[4,384,128]{2,1,0:T(8,128)(2,1)S(1)}, u32[]{:S(2)}, u32[]{:S(2)}) collective-permute-start(bf16[4,384,128]{2,1,0:T(8,128)(2,1)S(1)} %get-tuple-element.22), channel_id=1, source_target_pairs={{0,1},{1,0},{2,3},{3,2},{4,5},{5,4},{6,7},{7,6},{8,9},{9,8},{10,11... | collective-permute-start | bytes 1179656 | tf_op jit(solution)/shard_map/ppermute | solution.py:216

commit v5 on v4

--- a/solution.py
+++ b/solution.py
@@ -98,8 +98,8 @@
 def project_kernel(split, mine_ref, partner_ref, *refs):
     parts, kept_ref, sent_ref = refs[:-2], refs[-2], refs[-1]
     core = lax.axis_index("dp") & 1
-    for n in range(len(parts) // split):
-        piece = parts[n * split : (n + 1) * split]
+    for n, (start, stop) in enumerate(zip(split, split[1:])):
+        piece = parts[start:stop]
         count, blocks, width, _ = piece[0].shape
         rhs = jnp.concatenate(
             [
@@ -119,10 +119,12 @@
                 out_ref[first + 1 - core] = pltpu.roll(tile, width, 1).astype(BF)
 
 
-def project(mine, partner, parts, split):
+def project(mine, partner, pieces):
     rows = mine.shape[0]
-    count, _, width, _ = parts[0].shape
-    tiles = len(parts) // split * count
+    count, _, width, _ = pieces[0][0].shape
+    tiles = len(pieces) * count
+    parts = [part for piece in pieces for part in piece]
+    split = [sum(len(piece) for piece in pieces[:n]) for n in range(len(pieces) + 1)]
     vmem = pl.BlockSpec(memory_space=pltpu.VMEM)
     out = jax.ShapeDtypeStruct((tiles, rows, 2 * width), BF)
     return pl.pallas_call(
@@ -160,10 +162,10 @@
         for t in range(4):
             b = lax.rem(second + t, 4)
             at = lax.select(core == 0, b * 4 + a, a * 4 + b)
-            kept = tile((kept1, kept2), r, b).astype(F32)
-            got = tile((got1, got2), t, a).astype(F32)
+            kept = tile((kept1, kept2), r, b)
+            got = tile((got1, got2), t, a)
             where = pl.ds(pl.multiple_of(at * width, width), width)
-            out_ref[:, where] = jnp.where(ours, kept, got).astype(BF)
+            out_ref[:, where] = jnp.where(ours, kept, got)
 
 
 def merge(kept1, kept2, got1, got2):
@@ -217,20 +219,21 @@
 
 
 def per_device(up_pre, mix_pre, ln_gain, mix_weight, mix_bias, out_weight):
-    slab = sent_to_all(out_weight.T, "sp", 16)
+    slab = lax.all_gather(out_weight.T, "sp")
+    own = sent_to_all(slab, "dp", 4, GROUPS)
+    before = moved(own, ring(1))
+    high1 = moved(own[:, 8:], ring(-1))
+    low1 = moved(own[:, :8], ring(-1))
     normed = norm(mix_pre[0], ln_gain[None])
     gated = gate(normed, up_pre[0], mix_weight, mix_bias)
+    high1, gated = lax.optimization_barrier((high1, gated))
+    high2 = moved(high1, ring(-1))
+    low2 = moved(before[:, :8], ring(1))
     partner = moved(gated, SWAP)
-    slab, partner = lax.optimization_barrier((slab, partner))
-    own = sent_to_all(slab, "dp", 4, GROUPS)
-    before = moved(own, ring(1))
-    after = moved(own, ring(-1))
-    low2 = moved(before[:, :8], ring(1))
-    high2 = moved(after[:, 8:], ring(-1))
-    kept1, sent1 = project(gated, partner, [own, after, before], 1)
+    kept1, sent1 = project(gated, partner, [(own,), (low1, high1), (before,)])
     got1 = moved(sent1, SWAP)
     low2, high2, kept1 = lax.optimization_barrier((low2, high2, kept1))
-    kept2, sent2 = project(gated, partner, [low2, high2], 2)
+    kept2, sent2 = project(gated, partner, [(low2, high2)])
     got2 = moved(sent2, SWAP)
     return merge(kept1, kept2, got1, got2)[None]
 

time: 107 us -> 117 us (1.093)
  blocking collectives: 37.3 us -> 44.2 us
  waiting for transfers between devices: 19.6 us -> 24.5 us
  local copies, waits for them, and re-layouts: 2.48 us -> 0.37 us
    all_gather x0 -> x1, blocking collectives: none -> 30.7 us  [per_device(): slab = lax.all_gather(out_weight.T, 'sp')]
    all_to_all x2 -> x1, blocking collectives: 37.3 us -> 13.6 us  [sent_to_all(): lax.all_to_all(jnp.broadcast_to(value[None], (length, *value.shape)), axi...]
    ppermute x7 -> x8, waiting for transfers between devices: 19.6 us -> 24.5 us  [moved(): return lax.ppermute(value, 'dp', pairs)]
    unnamed x12 -> x10, local copies, waits for them, and re-layouts: 2.12 us -> 0.03 us
    ppermute x7 -> x8, starting transfers between devices: 36 us -> 36.3 us  [moved(): return lax.ppermute(value, 'dp', pairs)]
  transfers between devices with their start and end apart: 7 -> 8, of which waited for: 5 -> 6; matrix products, arithmetic and copies ran while one was open for 0% -> 0% of each run, Pallas kernels for 1% -> 5%
where the time goes in v5:
time: 117 us; the launch traced here: 116 us
  blocking collectives  44.2 us (38%)
  starting transfers between devices  36.3 us (31%)
  waiting for transfers between devices  24.5 us (21%)
  Pallas kernels  10.6 us (9%)
    ppermute x8, starting transfers between devices, moved(): return lax.ppermute(value, 'dp', pairs)  36.3 us
    all_gather x1, blocking collectives, per_device(): slab = lax.all_gather(out_weight.T, 'sp')  30.7 us
    ppermute x8, waiting for transfers between devices, moved(): return lax.ppermute(value, 'dp', pairs)  24.5 us
    all_to_all x1, blocking collectives, sent_to_all(): lax.all_to_all(jnp.broadcast_to(value[None], (length, *value.shape)), axi...  13.6 us
    pallas_call x2, Pallas kernels, project(): pl.pallas_call(functools.partial(project_kernel, split), in_specs=[vmem]...  3.8 us
    pallas_call x1, Pallas kernels, norm(): pl.pallas_call(norm_kernel, grid=(rows // BLOCK,), in_specs=[pl.BlockSpec...  3.08 us
  transfers between devices with their start and end apart: 8, of which 6 were waited for; matrix products, arithmetic and copies ran while one was open for 0% of the time, Pallas kernels for 5%

profile of v5, /device:TPU:1, one launch (start us, length us, event | category | flops | bytes accessed | tf_op | source)
XLA Modules:
  0.0 116.1 jit_solution(12039025041825280030)
XLA Ops:
  0.0 30.7 %all-gather = bf16[1024,128]{1,0:T(8,128)(2,1)S(1)} all-gather(bf16[64,128]{1,0:T(8,128)(2,1)} %bitcast.10), channel_id=2, replica_groups=mesh['sp'=16,'dp'=32] {'sp'}, dimensions={0}, use_global_device_ids=true | all-gather | bytes 278528 | tf_op jit(solution)/shard_map/all_gather | solution.py:222
  30.7 0.2 broadcast_in_dim.12
  30.9 13.6 %all_to_all.5.refs_0_ = bf16[4,16,64,128]{3,2,1,0:T(8,128)(2,1)S(1)} all-to-all(bf16[4,16,64,128]{3,2,1,0:T(8,128)(2,1)S(1)} %broadcast_in_dim.12), channel_id=1, replica_groups={{0,8,16,24},{2,10,18,26},{4,12,20,28},{6,14,22,30},{1,3,5,7},{9,11,13,1..., dimensions={0} | all-to-all | bytes 2097152 | tf_op jit(solution)/shard_map/all_to_all | solution.py:207
  44.5 0.1 fusion
  44.6 4.8 %collective-permute-start.2 = (bf16[4,8,64,128]{3,2,1,0:T(8,128)(2,1)S(1)}, bf16[4,8,64,128]{3,2,1,0:T(8,128)(2,1)S(1)}, u32[]{:S(2)}, u32[]{:S(2)}) collective-permute-start(bf16[4,8,64,128]{3,2,1,0:T(8,128)(2,1)S(1)} %get-tuple-element.24), channel_id=1, source_target_pairs={{0,6},{1,25},{2,0},{3,27},{4,2},{5,29},{6,4},{7,31},{8,14},{9,1},{... | collective-permute-start | bytes 1572872 | tf_op jit(solution)/shard_map/ppermute | solution.py:218
  49.4 0.0 copy-start.4
  49.4 3.1 %norm.1.normed_ref = bf16[384,2048]{1,0:T(8,128)(2,1)S(1)} custom-call(bf16[384,2048]{1,0:T(8,128)(2,1)S(1)} %bitcast.6, f32[1,2048]{1,0:T(1,128)S(1)} %bitcast.8), custom_call_target="tpu_custom_call" | custom-call | flops 4000000000 | bytes 3145728 | tf_op jit(solution)/shard_map/norm/pallas_call | solution.py:42
  52.5 1.7 %gate.1.mine_ref = bf16[384,2048]{1,0:T(8,128)(2,1)S(1)} custom-call(bf16[384,2048]{1,0:T(8,128)(2,1)S(1)} %norm.1.normed_ref, bf16[384,2048]{1,0:T(8,128)(2,1)S(1)} %bitcast.7, bf16[16,128,128]{2,1,0:T(8,128)(2,1)S(1)} %copy-done.2, f32[16,128]{1,0:T(8,128)S(1)} %copy-done.4), custom_call_target="tpu_custom_call" | custom-call | flops 4000000000 | bytes 4718592 | tf_op jit(solution)/shard_map/gate/pallas_call | solution.py:79
  54.2 3.1 %collective-permute-done.2.refs_2_ = bf16[4,8,64,128]{3,2,1,0:T(8,128)(2,1)S(1)} collective-permute-done((bf16[4,8,64,128]{3,2,1,0:T(8,128)(2,1)S(1)}, bf16[4,8,64,128]{3,2,1,0:T(8,128)(2,1)S(1)}, u32[]{:S(2)}, u32[]{:S(2)}) %collective-permute-start.2) | collective-permute-done | bytes 524320 | tf_op jit(solution)/shard_map/ppermute | solution.py:218
  57.4 12.2 %collective-permute-start.4 = (bf16[384,2048]{1,0:T(8,128)(2,1)S(1)}, bf16[384,2048]{1,0:T(8,128)(2,1)S(1)}, u32[]{:S(2)}, u32[]{:S(2)}) collective-permute-start(bf16[384,2048]{1,0:T(8,128)(2,1)S(1)} %gate.1.mine_ref), channel_id=1, source_target_pairs={{0,1},{1,0},{2,3},{3,2},{4,5},{5,4},{6,7},{7,6},{8,9},{9,8},{10,11... | collective-permute-start | bytes 4718600 | tf_op jit(solution)/shard_map/ppermute | solution.py:218
  69.5 3.9 %collective-permute-start = (bf16[4,16,64,128]{3,2,1,0:T(8,128)(2,1)S(1)}, bf16[4,16,64,128]{3,2,1,0:T(8,128)(2,1)S(1)}, u32[]{:S(2)}, u32[]{:S(2)}) collective-permute-start(bf16[4,16,64,128]{3,2,1,0:T(8,128)(2,1)S(1)} %all_to_all.5.refs_0_), channel_id=1, source_target_pairs={{0,2},{1,9},{2,4},{3,11},{4,6},{5,13},{6,0},{7,15},{8,10},{9,17},{... | collective-permute-start | bytes 3145736 | tf_op jit(solution)/shard_map/ppermute | solution.py:218
  73.4 3.0 %collective-permute-start.5 = (bf16[4,8,64,128]{3,2,1,0:T(8,128)(2,1)S(1)}, bf16[4,8,64,128]{3,2,1,0:T(8,128)(2,1)S(1)}, u32[]{:S(2)}, u32[]{:S(2)}) collective-permute-start(bf16[4,8,64,128]{3,2,1,0:T(8,128)(2,1)S(1)} %get-tuple-element.23), channel_id=1, source_target_pairs={{0,6},{1,25},{2,0},{3,27},{4,2},{5,29},{6,4},{7,31},{8,14},{9,1},{... | collective-permute-start | bytes 1572872 | tf_op jit(solution)/shard_map/ppermute | solution.py:218
  76.5 7.2 %collective-permute-done.5.refs_1_ = bf16[4,8,64,128]{3,2,1,0:T(8,128)(2,1)S(1)} collective-permute-done((bf16[4,8,64,128]{3,2,1,0:T(8,128)(2,1)S(1)}, bf16[4,8,64,128]{3,2,1,0:T(8,128)(2,1)S(1)}, u32[]{:S(2)}, u32[]{:S(2)}) %collective-permute-start.5) | collective-permute-done | bytes 524320 | tf_op jit(solution)/shard_map/ppermute | solution.py:218
  83.6 3.4 %collective-permute-done.refs_3_ = bf16[4,16,64,128]{3,2,1,0:T(8,128)(2,1)S(1)} collective-permute-done((bf16[4,16,64,128]{3,2,1,0:T(8,128)(2,1)S(1)}, bf16[4,16,64,128]{3,2,1,0:T(8,128)(2,1)S(1)}, u32[]{:S(2)}, u32[]{:S(2)}) %collective-permute-start) | collective-permute-done | bytes 1048608 | tf_op jit(solution)/shard_map/ppermute | solution.py:218
  87.0 2.7 %project.2 = (bf16[12,384,128]{2,1,0:T(8,128)(2,1)S(1)}, bf16[12,384,128]{2,1,0:T(8,128)(2,1)S(1)}) custom-call(bf16[384,2048]{1,0:T(8,128)(2,1)S(1)} %gate.1.mine_ref, bf16[384,2048]{1,0:T(8,128)(2,1)S(1)} %collective-permute-done.4.partner_ref, bf16[4,16,64,128]{3,2,1,0:T(8,128)(2,1)S(1)} %all_to_all.5.refs_0_, ...), custom_call_target="tpu_custom_call" | custom-call | flops 2415919104 | bytes 4194304 | tf_op jit(solution)/shard_map/project/pallas_call | solution.py:130
  89.7 2.8 %collective-permute-start.6 = (bf16[12,384,128]{2,1,0:T(8,128)(2,1)S(1)}, bf16[12,384,128]{2,1,0:T(8,128)(2,1)S(1)}, u32[]{:S(2)}, u32[]{:S(2)}) collective-permute-start(bf16[12,384,128]{2,1,0:T(8,128)(2,1)S(1)} %get-tuple-element.21), channel_id=1, source_target_pairs={{0,1},{1,0},{2,3},{3,2},{4,5},{5,4},{6,7},{7,6},{8,9},{9,8},{10,11... | collective-permute-start | bytes 3538952 | tf_op jit(solution)/shard_map/ppermute | solution.py:218
  92.5 5.0 %collective-permute-start.3 = (bf16[4,8,64,128]{3,2,1,0:T(8,128)(2,1)S(1)}, bf16[4,8,64,128]{3,2,1,0:T(8,128)(2,1)S(1)}, u32[]{:S(2)}, u32[]{:S(2)}) collective-permute-start(bf16[4,8,64,128]{3,2,1,0:T(8,128)(2,1)S(1)} %collective-permute-done.2.refs_2_), channel_id=1, source_target_pairs={{0,6},{1,25},{2,0},{3,27},{4,2},{5,29},{6,4},{7,31},{8,14},{9,1},{... | collective-permute-start | bytes 1572872 | tf_op jit(solution)/shard_map/ppermute | solution.py:218
  97.6 1.9 %collective-permute-start.1 = (bf16[4,8,64,128]{3,2,1,0:T(8,128)(2,1)S(1)}, bf16[4,8,64,128]{3,2,1,0:T(8,128)(2,1)S(1)}, u32[]{:S(2)}, u32[]{:S(2)}) collective-permute-start(bf16[4,8,64,128]{3,2,1,0:T(8,128)(2,1)S(1)} %slice.12), channel_id=1, source_target_pairs={{0,2},{1,9},{2,4},{3,11},{4,6},{5,13},{6,0},{7,15},{8,10},{9,17},{... | collective-permute-start | bytes 1572872 | tf_op jit(solution)/shard_map/ppermute | solution.py:218
  99.5 4.1 %collective-permute-done.3.refs_1_ = bf16[4,8,64,128]{3,2,1,0:T(8,128)(2,1)S(1)} collective-permute-done((bf16[4,8,64,128]{3,2,1,0:T(8,128)(2,1)S(1)}, bf16[4,8,64,128]{3,2,1,0:T(8,128)(2,1)S(1)}, u32[]{:S(2)}, u32[]{:S(2)}) %collective-permute-start.3) | collective-permute-done | bytes 524320 | tf_op jit(solution)/shard_map/ppermute | solution.py:218
  103.7 5.4 %collective-permute-done.1.refs_0_ = bf16[4,8,64,128]{3,2,1,0:T(8,128)(2,1)S(1)} collective-permute-done((bf16[4,8,64,128]{3,2,1,0:T(8,128)(2,1)S(1)}, bf16[4,8,64,128]{3,2,1,0:T(8,128)(2,1)S(1)}, u32[]{:S(2)}, u32[]{:S(2)}) %collective-permute-start.1) | collective-permute-done | bytes 524320 | tf_op jit(solution)/shard_map/ppermute | solution.py:218
  109.0 1.1 project.3
  110.1 2.7 %collective-permute-start.7 = (bf16[4,384,128]{2,1,0:T(8,128)(2,1)S(1)}, bf16[4,384,128]{2,1,0:T(8,128)(2,1)S(1)}, u32[]{:S(2)}, u32[]{:S(2)}) collective-permute-start(bf16[4,384,128]{2,1,0:T(8,128)(2,1)S(1)} %get-tuple-element.22), channel_id=1, source_target_pairs={{0,1},{1,0},{2,3},{3,2},{4,5},{5,4},{6,7},{7,6},{8,9},{9,8},{10,11... | collective-permute-start | bytes 1179656 | tf_op jit(solution)/shard_map/ppermute | solution.py:218
  112.8 1.3 %collective-permute-done.7.got2 = bf16[4,384,128]{2,1,0:T(8,128)(2,1)S(1)} collective-permute-done((bf16[4,384,128]{2,1,0:T(8,128)(2,1)S(1)}, bf16[4,384,128]{2,1,0:T(8,128)(2,1)S(1)}, u32[]{:S(2)}, u32[]{:S(2)}) %collective-permute-start.7) | collective-permute-done | bytes 393248 | tf_op jit(solution)/shard_map/ppermute | solution.py:218
  114.1 2.0 %merge.1 = bf16[384,2048]{1,0:T(8,128)(2,1)} custom-call(bf16[12,384,128]{2,1,0:T(8,128)(2,1)S(1)} %get-tuple-element.17.kept1, bf16[4,384,128]{2,1,0:T(8,128)(2,1)S(1)} %get-tuple-element.20.kept2, bf16[12,384,128]{2,1,0:T(8,128)(2,1)S(1)} %collective-permute-done.6.got1, bf16[4,384,128]{2,1,0:T(8,128)(2,1)S(1)} %collective-permute-done.7.got2), custom_call_target="tpu_custom_call" | custom-call | tf_op jit(solution)/shard_map/merge/pallas_call | solution.py:174
  (12 shorter events, 0.1 us)
Async XLA Ops:
  44.5 4.9 %copy-start = (bf16[1,384,2048]{2,1,0:T(8,128)(2,1)S(1)}, bf16[1,384,2048]{2,1,0:T(8,128)(2,1)}, u32[]{:S(2)}) copy-start(bf16[1,384,2048]{2,1,0:T(8,128)(2,1)} %param.7) | copy-start | bytes 4718596
  44.5 4.9 %copy-start.3 = (f32[2048]{0:T(1024)S(1)}, f32[2048]{0:T(1024)}, u32[]{:S(2)}) copy-start(f32[2048]{0:T(1024)} %param.8) | copy-start | bytes 24580
  44.6 12.8 %collective-permute-start.2 = (bf16[4,8,64,128]{3,2,1,0:T(8,128)(2,1)S(1)}, bf16[4,8,64,128]{3,2,1,0:T(8,128)(2,1)S(1)}, u32[]{:S(2)}, u32[]{:S(2)}) collective-permute-start(bf16[4,8,64,128]{3,2,1,0:T(8,128)(2,1)S(1)} %get-tuple-element.24), channel_id=1, source_target_pairs={{0,6},{1,25},{2,0},{3,27},{4,2},{5,29},{6,4},{7,31},{8,14},{9,1},{... | collective-permute-start | bytes 1572872 | tf_op jit(solution)/shard_map/ppermute | solution.py:218
  49.4 3.1 %copy-start.1 = (bf16[1,384,2048]{2,1,0:T(8,128)(2,1)S(1)}, bf16[1,384,2048]{2,1,0:T(8,128)(2,1)}, u32[]{:S(2)}) copy-start(bf16[1,384,2048]{2,1,0:T(8,128)(2,1)} %param.6) | copy-start | bytes 4718596
  49.4 3.1 %copy-start.2 = (bf16[16,128,128]{2,1,0:T(8,128)(2,1)S(1)}, bf16[16,128,128]{2,1,0:T(8,128)(2,1)}, u32[]{:S(2)}) copy-start(bf16[16,128,128]{2,1,0:T(8,128)(2,1)} %weight_ref.1) | copy-start | bytes 1572868
  49.4 3.1 %copy-start.4 = (f32[16,128]{1,0:T(8,128)S(1)}, f32[16,128]{1,0:T(8,128)}, u32[]{:S(2)}) copy-start(f32[16,128]{1,0:T(8,128)} %bias_ref.1) | copy-start | bytes 24580
  57.4 29.6 %collective-permute-start.4 = (bf16[384,2048]{1,0:T(8,128)(2,1)S(1)}, bf16[384,2048]{1,0:T(8,128)(2,1)S(1)}, u32[]{:S(2)}, u32[]{:S(2)}) collective-permute-start(bf16[384,2048]{1,0:T(8,128)(2,1)S(1)} %gate.1.mine_ref), channel_id=1, source_target_pairs={{0,1},{1,0},{2,3},{3,2},{4,5},{5,4},{6,7},{7,6},{8,9},{9,8},{10,11... | collective-permute-start | bytes 4718600 | tf_op jit(solution)/shard_map/ppermute | solution.py:218
  69.5 17.5 %collective-permute-start = (bf16[4,16,64,128]{3,2,1,0:T(8,128)(2,1)S(1)}, bf16[4,16,64,128]{3,2,1,0:T(8,128)(2,1)S(1)}, u32[]{:S(2)}, u32[]{:S(2)}) collective-permute-start(bf16[4,16,64,128]{3,2,1,0:T(8,128)(2,1)S(1)} %all_to_all.5.refs_0_), channel_id=1, source_target_pairs={{0,2},{1,9},{2,4},{3,11},{4,6},{5,13},{6,0},{7,15},{8,10},{9,17},{... | collective-permute-start | bytes 3145736 | tf_op jit(solution)/shard_map/ppermute | solution.py:218
  73.4 10.2 %collective-permute-start.5 = (bf16[4,8,64,128]{3,2,1,0:T(8,128)(2,1)S(1)}, bf16[4,8,64,128]{3,2,1,0:T(8,128)(2,1)S(1)}, u32[]{:S(2)}, u32[]{:S(2)}) collective-permute-start(bf16[4,8,64,128]{3,2,1,0:T(8,128)(2,1)S(1)} %get-tuple-element.23), channel_id=1, source_target_pairs={{0,6},{1,25},{2,0},{3,27},{4,2},{5,29},{6,4},{7,31},{8,14},{9,1},{... | collective-permute-start | bytes 1572872 | tf_op jit(solution)/shard_map/ppermute | solution.py:218
  89.7 24.4 %collective-permute-start.6 = (bf16[12,384,128]{2,1,0:T(8,128)(2,1)S(1)}, bf16[12,384,128]{2,1,0:T(8,128)(2,1)S(1)}, u32[]{:S(2)}, u32[]{:S(2)}) collective-permute-start(bf16[12,384,128]{2,1,0:T(8,128)(2,1)S(1)} %get-tuple-element.21), channel_id=1, source_target_pairs={{0,1},{1,0},{2,3},{3,2},{4,5},{5,4},{6,7},{7,6},{8,9},{9,8},{10,11... | collective-permute-start | bytes 3538952 | tf_op jit(solution)/shard_map/ppermute | solution.py:218
  92.5 11.1 %collective-permute-start.3 = (bf16[4,8,64,128]{3,2,1,0:T(8,128)(2,1)S(1)}, bf16[4,8,64,128]{3,2,1,0:T(8,128)(2,1)S(1)}, u32[]{:S(2)}, u32[]{:S(2)}) collective-permute-start(bf16[4,8,64,128]{3,2,1,0:T(8,128)(2,1)S(1)} %collective-permute-done.2.refs_2_), channel_id=1, source_target_pairs={{0,6},{1,25},{2,0},{3,27},{4,2},{5,29},{6,4},{7,31},{8,14},{9,1},{... | collective-permute-start | bytes 1572872 | tf_op jit(solution)/shard_map/ppermute | solution.py:218
  97.6 11.4 %collective-permute-start.1 = (bf16[4,8,64,128]{3,2,1,0:T(8,128)(2,1)S(1)}, bf16[4,8,64,128]{3,2,1,0:T(8,128)(2,1)S(1)}, u32[]{:S(2)}, u32[]{:S(2)}) collective-permute-start(bf16[4,8,64,128]{3,2,1,0:T(8,128)(2,1)S(1)} %slice.12), channel_id=1, source_target_pairs={{0,2},{1,9},{2,4},{3,11},{4,6},{5,13},{6,0},{7,15},{8,10},{9,17},{... | collective-permute-start | bytes 1572872 | tf_op jit(solution)/shard_map/ppermute | solution.py:218
  110.1 4.0 %collective-permute-start.7 = (bf16[4,384,128]{2,1,0:T(8,128)(2,1)S(1)}, bf16[4,384,128]{2,1,0:T(8,128)(2,1)S(1)}, u32[]{:S(2)}, u32[]{:S(2)}) collective-permute-start(bf16[4,384,128]{2,1,0:T(8,128)(2,1)S(1)} %get-tuple-element.22), channel_id=1, source_target_pairs={{0,1},{1,0},{2,3},{3,2},{4,5},{5,4},{6,7},{7,6},{8,9},{9,8},{10,11... | collective-permute-start | bytes 1179656 | tf_op jit(solution)/shard_map/ppermute | solution.py:218

commit v6 on v5

--- a/solution.py
+++ b/solution.py
@@ -219,18 +219,19 @@
 
 
 def per_device(up_pre, mix_pre, ln_gain, mix_weight, mix_bias, out_weight):
-    slab = lax.all_gather(out_weight.T, "sp")
-    own = sent_to_all(slab, "dp", 4, GROUPS)
-    before = moved(own, ring(1))
-    high1 = moved(own[:, 8:], ring(-1))
-    low1 = moved(own[:, :8], ring(-1))
+    slab = sent_to_all(out_weight.T, "sp", 16)
     normed = norm(mix_pre[0], ln_gain[None])
     gated = gate(normed, up_pre[0], mix_weight, mix_bias)
-    high1, gated = lax.optimization_barrier((high1, gated))
+    partner = moved(gated, SWAP)
+    slab, partner = lax.optimization_barrier((slab, partner))
+    own = sent_to_all(slab, "dp", 4, GROUPS)
+    low3 = moved(own[:, :8], ring(1))
+    high1 = moved(own[:, 8:], ring(-1))
+    high3 = moved(own[:, 8:], ring(1))
+    low1 = moved(own[:, :8], ring(-1))
+    low2 = moved(low3, ring(1))
     high2 = moved(high1, ring(-1))
-    low2 = moved(before[:, :8], ring(1))
-    partner = moved(gated, SWAP)
-    kept1, sent1 = project(gated, partner, [(own,), (low1, high1), (before,)])
+    kept1, sent1 = project(gated, partner, [(own,), (low1, high1), (low3, high3)])
     got1 = moved(sent1, SWAP)
     low2, high2, kept1 = lax.optimization_barrier((low2, high2, kept1))
     kept2, sent2 = project(gated, partner, [(low2, high2)])

time: 117 us -> 108 us (0.923)
  waiting for transfers between devices: 24.5 us -> 16.6 us
  blocking collectives: 44.2 us -> 37.3 us
  starting transfers between devices: 36.3 us -> 40.6 us
  local copies, waits for them, and re-layouts: 0.37 us -> 2.48 us
    all_gather x1 -> x0, blocking collectives: 30.7 us -> none  [per_device(): slab = lax.all_gather(out_weight.T, 'sp')]
    all_to_all x1 -> x2, blocking collectives: 13.6 us -> 37.3 us  [sent_to_all(): lax.all_to_all(jnp.broadcast_to(value[None], (length, *value.shape)), axi...]
    ppermute x8 -> x9, waiting for transfers between devices: 24.5 us -> 16.6 us  [moved(): return lax.ppermute(value, 'dp', pairs)]
    ppermute x8 -> x9, starting transfers between devices: 36.3 us -> 40.6 us  [moved(): return lax.ppermute(value, 'dp', pairs)]
    unnamed x10 -> x12, local copies, waits for them, and re-layouts: 0.03 us -> 2.12 us
  transfers between devices with their start and end apart: 8 -> 9, of which waited for: 6 -> 6; matrix products, arithmetic and copies ran while one was open for 0% -> 0% of each run, Pallas kernels for 5% -> 1%
where the time goes in v6:
time: 108 us
  starting transfers between devices  40.6 us (38%)
  blocking collectives  37.3 us (35%)
  waiting for transfers between devices  16.6 us (15%)
  Pallas kernels  10.6 us (10%)
  local copies, waits for them, and re-layouts  2.48 us (2%)
    ppermute x9, starting transfers between devices, moved(): return lax.ppermute(value, 'dp', pairs)  40.6 us
    all_to_all x2, blocking collectives, sent_to_all(): lax.all_to_all(jnp.broadcast_to(value[None], (length, *value.shape)), axi...  37.3 us
    ppermute x9, waiting for transfers between devices, moved(): return lax.ppermute(value, 'dp', pairs)  16.6 us
    pallas_call x2, Pallas kernels, project(): pl.pallas_call(functools.partial(project_kernel, split), in_specs=[vmem]...  3.78 us
    pallas_call x1, Pallas kernels, norm(): pl.pallas_call(norm_kernel, grid=(rows // BLOCK,), in_specs=[pl.BlockSpec...  3.06 us
  transfers between devices with their start and end apart: 9, of which 6 were waited for; matrix products, arithmetic and copies ran while one was open for 0% of the time, Pallas kernels for 1%

profile of v6, /device:TPU:1, one launch (start us, length us, event | category | flops | bytes accessed | tf_op | source)
XLA Modules:
  0.0 107.7 jit_solution(8961131618363819510)
XLA Ops:
  0.0 1.4 %copy-done = bf16[1,384,2048]{2,1,0:T(8,128)(2,1)S(1)} copy-done((bf16[1,384,2048]{2,1,0:T(8,128)(2,1)S(1)}, bf16[1,384,2048]{2,1,0:T(8,128)(2,1)}, u32[]{:S(2)}) %copy-start) | copy-done | bytes 1572888
  1.4 0.7 copy-done.3
  2.1 3.1 %norm.1.normed_ref = bf16[384,2048]{1,0:T(8,128)(2,1)S(1)} custom-call(bf16[384,2048]{1,0:T(8,128)(2,1)S(1)} %bitcast.5, f32[1,2048]{1,0:T(1,128)S(1)} %bitcast.7), custom_call_target="tpu_custom_call" | custom-call | flops 4000000000 | bytes 3145728 | tf_op jit(solution)/shard_map/norm/pallas_call | solution.py:42
  5.2 1.7 %gate.1.mine_ref = bf16[384,2048]{1,0:T(8,128)(2,1)S(1)} custom-call(bf16[384,2048]{1,0:T(8,128)(2,1)S(1)} %norm.1.normed_ref, bf16[384,2048]{1,0:T(8,128)(2,1)S(1)} %bitcast.6, bf16[16,128,128]{2,1,0:T(8,128)(2,1)S(1)} %copy-done.2, f32[16,128]{1,0:T(8,128)S(1)} %copy-done.4), custom_call_target="tpu_custom_call" | custom-call | flops 4000000000 | bytes 4718592 | tf_op jit(solution)/shard_map/gate/pallas_call | solution.py:79
  6.9 8.7 %collective-permute-start = (bf16[384,2048]{1,0:T(8,128)(2,1)S(1)}, bf16[384,2048]{1,0:T(8,128)(2,1)S(1)}, u32[]{:S(2)}, u32[]{:S(2)}) collective-permute-start(bf16[384,2048]{1,0:T(8,128)(2,1)S(1)} %gate.1.mine_ref), channel_id=1, source_target_pairs={{0,1},{1,0},{2,3},{3,2},{4,5},{5,4},{6,7},{7,6},{8,9},{9,8},{10,11... | collective-permute-start | bytes 4718600 | tf_op jit(solution)/shard_map/ppermute | solution.py:218
  15.8 23.7 %all_to_all.10 = bf16[16,64,128]{2,1,0:T(8,128)(2,1)S(1)} all-to-all(bf16[16,64,128]{2,1,0:T(8,128)(2,1)S(1)} %broadcast_in_dim.8), channel_id=1, replica_groups=mesh['sp'=16,'dp'=32] {'sp'}, dimensions={0} | all-to-all | bytes 524288 | tf_op jit(solution)/shard_map/all_to_all | solution.py:207
  39.7 13.6 %all_to_all.11.refs_0_ = bf16[4,16,64,128]{3,2,1,0:T(8,128)(2,1)S(1)} all-to-all(bf16[4,16,64,128]{3,2,1,0:T(8,128)(2,1)S(1)} %broadcast_in_dim.20), channel_id=1, replica_groups={{0,8,16,24},{2,10,18,26},{4,12,20,28},{6,14,22,30},{1,3,5,7},{9,11,13,1..., dimensions={0} | all-to-all | bytes 2097152 | tf_op jit(solution)/shard_map/all_to_all | solution.py:207
  53.4 3.2 %collective-permute-start.1 = (bf16[4,8,64,128]{3,2,1,0:T(8,128)(2,1)S(1)}, bf16[4,8,64,128]{3,2,1,0:T(8,128)(2,1)S(1)}, u32[]{:S(2)}, u32[]{:S(2)}) collective-permute-start(bf16[4,8,64,128]{3,2,1,0:T(8,128)(2,1)S(1)} %get-tuple-element.24), channel_id=1, source_target_pairs={{0,2},{1,9},{2,4},{3,11},{4,6},{5,13},{6,0},{7,15},{8,10},{9,17},{... | collective-permute-start | bytes 1572872 | tf_op jit(solution)/shard_map/ppermute | solution.py:218
  56.6 3.7 %collective-permute-start.3 = (bf16[4,8,64,128]{3,2,1,0:T(8,128)(2,1)S(1)}, bf16[4,8,64,128]{3,2,1,0:T(8,128)(2,1)S(1)}, u32[]{:S(2)}, u32[]{:S(2)}) collective-permute-start(bf16[4,8,64,128]{3,2,1,0:T(8,128)(2,1)S(1)} %get-tuple-element.23), channel_id=1, source_target_pairs={{0,6},{1,25},{2,0},{3,27},{4,2},{5,29},{6,4},{7,31},{8,14},{9,1},{... | collective-permute-start | bytes 1572872 | tf_op jit(solution)/shard_map/ppermute | solution.py:218
  60.2 3.4 %collective-permute-start.5 = (bf16[4,8,64,128]{3,2,1,0:T(8,128)(2,1)S(1)}, bf16[4,8,64,128]{3,2,1,0:T(8,128)(2,1)S(1)}, u32[]{:S(2)}, u32[]{:S(2)}) collective-permute-start(bf16[4,8,64,128]{3,2,1,0:T(8,128)(2,1)S(1)} %get-tuple-element.24), channel_id=1, source_target_pairs={{0,6},{1,25},{2,0},{3,27},{4,2},{5,29},{6,4},{7,31},{8,14},{9,1},{... | collective-permute-start | bytes 1572872 | tf_op jit(solution)/shard_map/ppermute | solution.py:218
  63.6 1.9 %collective-permute-start.6 = (bf16[4,8,64,128]{3,2,1,0:T(8,128)(2,1)S(1)}, bf16[4,8,64,128]{3,2,1,0:T(8,128)(2,1)S(1)}, u32[]{:S(2)}, u32[]{:S(2)}) collective-permute-start(bf16[4,8,64,128]{3,2,1,0:T(8,128)(2,1)S(1)} %get-tuple-element.23), channel_id=1, source_target_pairs={{0,2},{1,9},{2,4},{3,11},{4,6},{5,13},{6,0},{7,15},{8,10},{9,17},{... | collective-permute-start | bytes 1572872 | tf_op jit(solution)/shard_map/ppermute | solution.py:218
  65.5 1.2 %collective-permute-done.3.refs_2_ = bf16[4,8,64,128]{3,2,1,0:T(8,128)(2,1)S(1)} collective-permute-done((bf16[4,8,64,128]{3,2,1,0:T(8,128)(2,1)S(1)}, bf16[4,8,64,128]{3,2,1,0:T(8,128)(2,1)S(1)}, u32[]{:S(2)}, u32[]{:S(2)}) %collective-permute-start.3) | collective-permute-done | bytes 524320 | tf_op jit(solution)/shard_map/ppermute | solution.py:218
  66.8 5.6 %collective-permute-done.5.refs_1_ = bf16[4,8,64,128]{3,2,1,0:T(8,128)(2,1)S(1)} collective-permute-done((bf16[4,8,64,128]{3,2,1,0:T(8,128)(2,1)S(1)}, bf16[4,8,64,128]{3,2,1,0:T(8,128)(2,1)S(1)}, u32[]{:S(2)}, u32[]{:S(2)}) %collective-permute-start.5) | collective-permute-done | bytes 524320 | tf_op jit(solution)/shard_map/ppermute | solution.py:218
  72.4 2.3 %collective-permute-done.6.refs_4_ = bf16[4,8,64,128]{3,2,1,0:T(8,128)(2,1)S(1)} collective-permute-done((bf16[4,8,64,128]{3,2,1,0:T(8,128)(2,1)S(1)}, bf16[4,8,64,128]{3,2,1,0:T(8,128)(2,1)S(1)}, u32[]{:S(2)}, u32[]{:S(2)}) %collective-permute-start.6) | collective-permute-done | bytes 524320 | tf_op jit(solution)/shard_map/ppermute | solution.py:218
  74.7 2.7 %project.2 = (bf16[12,384,128]{2,1,0:T(8,128)(2,1)S(1)}, bf16[12,384,128]{2,1,0:T(8,128)(2,1)S(1)}) custom-call(bf16[384,2048]{1,0:T(8,128)(2,1)S(1)} %gate.1.mine_ref, bf16[384,2048]{1,0:T(8,128)(2,1)S(1)} %collective-permute-done.partner_ref, bf16[4,16,64,128]{3,2,1,0:T(8,128)(2,1)S(1)} %all_to_all.11.refs_0_, ...), custom_call_target="tpu_custom_call" | custom-call | flops 2415919104 | bytes 4194304 | tf_op jit(solution)/shard_map/project/pallas_call | solution.py:130
  77.5 10.2 %collective-permute-start.7 = (bf16[12,384,128]{2,1,0:T(8,128)(2,1)S(1)}, bf16[12,384,128]{2,1,0:T(8,128)(2,1)S(1)}, u32[]{:S(2)}, u32[]{:S(2)}) collective-permute-start(bf16[12,384,128]{2,1,0:T(8,128)(2,1)S(1)} %get-tuple-element.21), channel_id=1, source_target_pairs={{0,1},{1,0},{2,3},{3,2},{4,5},{5,4},{6,7},{7,6},{8,9},{9,8},{10,11... | collective-permute-start | bytes 3538952 | tf_op jit(solution)/shard_map/ppermute | solution.py:218
  87.6 1.9 %collective-permute-start.2 = (bf16[4,8,64,128]{3,2,1,0:T(8,128)(2,1)S(1)}, bf16[4,8,64,128]{3,2,1,0:T(8,128)(2,1)S(1)}, u32[]{:S(2)}, u32[]{:S(2)}) collective-permute-start(bf16[4,8,64,128]{3,2,1,0:T(8,128)(2,1)S(1)} %collective-permute-done.1.refs_3_), channel_id=1, source_target_pairs={{0,2},{1,9},{2,4},{3,11},{4,6},{5,13},{6,0},{7,15},{8,10},{9,17},{... | collective-permute-start | bytes 1572872 | tf_op jit(solution)/shard_map/ppermute | solution.py:218
  89.6 4.6 %collective-permute-start.4 = (bf16[4,8,64,128]{3,2,1,0:T(8,128)(2,1)S(1)}, bf16[4,8,64,128]{3,2,1,0:T(8,128)(2,1)S(1)}, u32[]{:S(2)}, u32[]{:S(2)}) collective-permute-start(bf16[4,8,64,128]{3,2,1,0:T(8,128)(2,1)S(1)} %collective-permute-done.3.refs_2_), channel_id=1, source_target_pairs={{0,6},{1,25},{2,0},{3,27},{4,2},{5,29},{6,4},{7,31},{8,14},{9,1},{... | collective-permute-start | bytes 1572872 | tf_op jit(solution)/shard_map/ppermute | solution.py:218
  94.1 4.9 %collective-permute-done.2.refs_0_ = bf16[4,8,64,128]{3,2,1,0:T(8,128)(2,1)S(1)} collective-permute-done((bf16[4,8,64,128]{3,2,1,0:T(8,128)(2,1)S(1)}, bf16[4,8,64,128]{3,2,1,0:T(8,128)(2,1)S(1)}, u32[]{:S(2)}, u32[]{:S(2)}) %collective-permute-start.2) | collective-permute-done | bytes 524320 | tf_op jit(solution)/shard_map/ppermute | solution.py:218
  99.1 1.2 %collective-permute-done.4.refs_1_ = bf16[4,8,64,128]{3,2,1,0:T(8,128)(2,1)S(1)} collective-permute-done((bf16[4,8,64,128]{3,2,1,0:T(8,128)(2,1)S(1)}, bf16[4,8,64,128]{3,2,1,0:T(8,128)(2,1)S(1)}, u32[]{:S(2)}, u32[]{:S(2)}) %collective-permute-start.4) | collective-permute-done | bytes 524320 | tf_op jit(solution)/shard_map/ppermute | solution.py:218
  100.2 1.1 %project.3 = (bf16[4,384,128]{2,1,0:T(8,128)(2,1)S(1)}, bf16[4,384,128]{2,1,0:T(8,128)(2,1)S(1)}) custom-call(bf16[384,2048]{1,0:T(8,128)(2,1)S(1)} %gate.1.mine_ref, bf16[384,2048]{1,0:T(8,128)(2,1)S(1)} %collective-permute-done.partner_ref, bf16[4,8,64,128]{3,2,1,0:T(8,128)(2,1)S(1)} %collective-permute-done.2.refs_0_, ...), custom_call_target="tpu_custom_call" | custom-call | flops 805306368 | bytes 4194304 | tf_op jit(solution)/shard_map/project/pallas_call | solution.py:130
  101.3 3.1 %collective-permute-start.8 = (bf16[4,384,128]{2,1,0:T(8,128)(2,1)S(1)}, bf16[4,384,128]{2,1,0:T(8,128)(2,1)S(1)}, u32[]{:S(2)}, u32[]{:S(2)}) collective-permute-start(bf16[4,384,128]{2,1,0:T(8,128)(2,1)S(1)} %get-tuple-element.22), channel_id=1, source_target_pairs={{0,1},{1,0},{2,3},{3,2},{4,5},{5,4},{6,7},{7,6},{8,9},{9,8},{10,11... | collective-permute-start | bytes 1179656 | tf_op jit(solution)/shard_map/ppermute | solution.py:218
  104.4 1.3 %collective-permute-done.8.got2 = bf16[4,384,128]{2,1,0:T(8,128)(2,1)S(1)} collective-permute-done((bf16[4,384,128]{2,1,0:T(8,128)(2,1)S(1)}, bf16[4,384,128]{2,1,0:T(8,128)(2,1)S(1)}, u32[]{:S(2)}, u32[]{:S(2)}) %collective-permute-start.8) | collective-permute-done | bytes 393248 | tf_op jit(solution)/shard_map/ppermute | solution.py:218
  105.7 2.0 %merge.1 = bf16[384,2048]{1,0:T(8,128)(2,1)} custom-call(bf16[12,384,128]{2,1,0:T(8,128)(2,1)S(1)} %get-tuple-element.17.kept1, bf16[4,384,128]{2,1,0:T(8,128)(2,1)S(1)} %get-tuple-element.20.kept2, bf16[12,384,128]{2,1,0:T(8,128)(2,1)S(1)} %collective-permute-done.7.got1, bf16[4,384,128]{2,1,0:T(8,128)(2,1)S(1)} %collective-permute-done.8.got2), custom_call_target="tpu_custom_call" | custom-call | tf_op jit(solution)/shard_map/merge/pallas_call | solution.py:174
  (16 shorter events, 0.4 us)
Async XLA Ops:
  0.0 1.4 %copy-start = (bf16[1,384,2048]{2,1,0:T(8,128)(2,1)S(1)}, bf16[1,384,2048]{2,1,0:T(8,128)(2,1)}, u32[]{:S(2)}) copy-start(bf16[1,384,2048]{2,1,0:T(8,128)(2,1)} %param.7) | copy-start | bytes 4718596
  1.4 0.7 copy-start.3
  2.1 3.1 %copy-start.1 = (bf16[1,384,2048]{2,1,0:T(8,128)(2,1)S(1)}, bf16[1,384,2048]{2,1,0:T(8,128)(2,1)}, u32[]{:S(2)}) copy-start(bf16[1,384,2048]{2,1,0:T(8,128)(2,1)} %param.6) | copy-start | bytes 4718596
  2.1 3.1 %copy-start.2 = (bf16[16,128,128]{2,1,0:T(8,128)(2,1)S(1)}, bf16[16,128,128]{2,1,0:T(8,128)(2,1)}, u32[]{:S(2)}) copy-start(bf16[16,128,128]{2,1,0:T(8,128)(2,1)} %weight_ref.1) | copy-start | bytes 1572868
  2.1 3.1 %copy-start.4 = (f32[16,128]{1,0:T(8,128)S(1)}, f32[16,128]{1,0:T(8,128)}, u32[]{:S(2)}) copy-start(f32[16,128]{1,0:T(8,128)} %bias_ref.1) | copy-start | bytes 24580
  5.2 10.5 %copy-start.5 = (bf16[128,64]{0,1:T(8,128)(2,1)S(1)}, bf16[128,64]{0,1:T(8,128)(2,1)}, u32[]{:S(2)}) copy-start(bf16[128,64]{0,1:T(8,128)(2,1)} %param.11) | copy-start | bytes 49156
  6.9 32.5 %collective-permute-start = (bf16[384,2048]{1,0:T(8,128)(2,1)S(1)}, bf16[384,2048]{1,0:T(8,128)(2,1)S(1)}, u32[]{:S(2)}, u32[]{:S(2)}) collective-permute-start(bf16[384,2048]{1,0:T(8,128)(2,1)S(1)} %gate.1.mine_ref), channel_id=1, source_target_pairs={{0,1},{1,0},{2,3},{3,2},{4,5},{5,4},{6,7},{7,6},{8,9},{9,8},{10,11... | collective-permute-start | bytes 4718600 | tf_op jit(solution)/shard_map/ppermute | solution.py:218
  53.4 12.2 %collective-permute-start.1 = (bf16[4,8,64,128]{3,2,1,0:T(8,128)(2,1)S(1)}, bf16[4,8,64,128]{3,2,1,0:T(8,128)(2,1)S(1)}, u32[]{:S(2)}, u32[]{:S(2)}) collective-permute-start(bf16[4,8,64,128]{3,2,1,0:T(8,128)(2,1)S(1)} %get-tuple-element.24), channel_id=1, source_target_pairs={{0,2},{1,9},{2,4},{3,11},{4,6},{5,13},{6,0},{7,15},{8,10},{9,17},{... | collective-permute-start | bytes 1572872 | tf_op jit(solution)/shard_map/ppermute | solution.py:218
  56.6 10.2 %collective-permute-start.3 = (bf16[4,8,64,128]{3,2,1,0:T(8,128)(2,1)S(1)}, bf16[4,8,64,128]{3,2,1,0:T(8,128)(2,1)S(1)}, u32[]{:S(2)}, u32[]{:S(2)}) collective-permute-start(bf16[4,8,64,128]{3,2,1,0:T(8,128)(2,1)S(1)} %get-tuple-element.23), channel_id=1, source_target_pairs={{0,6},{1,25},{2,0},{3,27},{4,2},{5,29},{6,4},{7,31},{8,14},{9,1},{... | collective-permute-start | bytes 1572872 | tf_op jit(solution)/shard_map/ppermute | solution.py:218
  60.2 12.2 %collective-permute-start.5 = (bf16[4,8,64,128]{3,2,1,0:T(8,128)(2,1)S(1)}, bf16[4,8,64,128]{3,2,1,0:T(8,128)(2,1)S(1)}, u32[]{:S(2)}, u32[]{:S(2)}) collective-permute-start(bf16[4,8,64,128]{3,2,1,0:T(8,128)(2,1)S(1)} %get-tuple-element.24), channel_id=1, source_target_pairs={{0,6},{1,25},{2,0},{3,27},{4,2},{5,29},{6,4},{7,31},{8,14},{9,1},{... | collective-permute-start | bytes 1572872 | tf_op jit(solution)/shard_map/ppermute | solution.py:218
  63.6 11.1 %collective-permute-start.6 = (bf16[4,8,64,128]{3,2,1,0:T(8,128)(2,1)S(1)}, bf16[4,8,64,128]{3,2,1,0:T(8,128)(2,1)S(1)}, u32[]{:S(2)}, u32[]{:S(2)}) collective-permute-start(bf16[4,8,64,128]{3,2,1,0:T(8,128)(2,1)S(1)} %get-tuple-element.23), channel_id=1, source_target_pairs={{0,2},{1,9},{2,4},{3,11},{4,6},{5,13},{6,0},{7,15},{8,10},{9,17},{... | collective-permute-start | bytes 1572872 | tf_op jit(solution)/shard_map/ppermute | solution.py:218
  77.5 28.3 %collective-permute-start.7 = (bf16[12,384,128]{2,1,0:T(8,128)(2,1)S(1)}, bf16[12,384,128]{2,1,0:T(8,128)(2,1)S(1)}, u32[]{:S(2)}, u32[]{:S(2)}) collective-permute-start(bf16[12,384,128]{2,1,0:T(8,128)(2,1)S(1)} %get-tuple-element.21), channel_id=1, source_target_pairs={{0,1},{1,0},{2,3},{3,2},{4,5},{5,4},{6,7},{7,6},{8,9},{9,8},{10,11... | collective-permute-start | bytes 3538952 | tf_op jit(solution)/shard_map/ppermute | solution.py:218
  87.6 11.4 %collective-permute-start.2 = (bf16[4,8,64,128]{3,2,1,0:T(8,128)(2,1)S(1)}, bf16[4,8,64,128]{3,2,1,0:T(8,128)(2,1)S(1)}, u32[]{:S(2)}, u32[]{:S(2)}) collective-permute-start(bf16[4,8,64,128]{3,2,1,0:T(8,128)(2,1)S(1)} %collective-permute-done.1.refs_3_), channel_id=1, source_target_pairs={{0,2},{1,9},{2,4},{3,11},{4,6},{5,13},{6,0},{7,15},{8,10},{9,17},{... | collective-permute-start | bytes 1572872 | tf_op jit(solution)/shard_map/ppermute | solution.py:218
  89.6 10.7 %collective-permute-start.4 = (bf16[4,8,64,128]{3,2,1,0:T(8,128)(2,1)S(1)}, bf16[4,8,64,128]{3,2,1,0:T(8,128)(2,1)S(1)}, u32[]{:S(2)}, u32[]{:S(2)}) collective-permute-start(bf16[4,8,64,128]{3,2,1,0:T(8,128)(2,1)S(1)} %collective-permute-done.3.refs_2_), channel_id=1, source_target_pairs={{0,6},{1,25},{2,0},{3,27},{4,2},{5,29},{6,4},{7,31},{8,14},{9,1},{... | collective-permute-start | bytes 1572872 | tf_op jit(solution)/shard_map/ppermute | solution.py:218
  101.3 4.4 %collective-permute-start.8 = (bf16[4,384,128]{2,1,0:T(8,128)(2,1)S(1)}, bf16[4,384,128]{2,1,0:T(8,128)(2,1)S(1)}, u32[]{:S(2)}, u32[]{:S(2)}) collective-permute-start(bf16[4,384,128]{2,1,0:T(8,128)(2,1)S(1)} %get-tuple-element.22), channel_id=1, source_target_pairs={{0,1},{1,0},{2,3},{3,2},{4,5},{5,4},{6,7},{7,6},{8,9},{9,8},{10,11... | collective-permute-start | bytes 1179656 | tf_op jit(solution)/shard_map/ppermute | solution.py:218
